TPU v7x, 512 devices: a whole 4x8x8 slice. The times are simulated.
512 devices in a mesh: sp: 128 (over z, y, core), tp: 4 (over x).
Axes of the slice: x: 4, y: 8, z: 8, core: 2. Of those that a mesh axis runs over, the one named last changes fastest.
Arguments:
- tokens: bfloat16 [65536, 2048], P('sp'), may hold values from -6 to 6
- norm_gain: bfloat16 [2048], replicated, may hold values from 0.099609375 to 1.8984375
- w_conv_value: bfloat16 [2048, 2048], P('sp', 'tp'), may hold values from -0.125 to 0.125
- w_conv_gate: bfloat16 [2048, 2048], P('sp', 'tp'), may hold values from -0.125 to 0.125
- w_query: bfloat16 [2048, 2048], P('sp', 'tp'), may hold values from -0.125 to 0.125
- w_key: bfloat16 [2048, 512], P('sp', 'tp'), may hold values from -0.125 to 0.125
- w_value: bfloat16 [2048, 512], P('sp', 'tp'), may hold values from -0.125 to 0.125
- conv_taps: float32 [31, 2048], P(None, 'tp'), as said below
- ln_gain: float32 [2048], P('tp'), may hold values from 0.1 to 1.9
- sinks: float32 [32], P('tp'), may hold values from 3 to 6
- out_conv: bfloat16 [2048, 2048], P('tp', 'sp'), may hold values from -0.125 to 0.125
- out_attn: bfloat16 [2048, 2048], P('tp', 'sp'), may hold values from -0.5 to 0.5
Outputs:
- mixed: bfloat16 [65536, 2048], P(('sp', 'tp'))
- log_sums: float32 [32, 65536], P('tp', 'sp')
Inputs may be any that keep to these rules, and one draw needn't show every extreme that they name: `conv_taps`: each tap lies within 30 / sqrt(31) in magnitude.
All inputs are finite; a program needn't handle non-finite values.
Results may differ from a plain program's by a relative error of at most 0.017.
Values may be sent and summed in bfloat16 or wider, within the bound.
A program may use at most 64 MiB of HBM per device.

v0:
```python
import jax
import jax.numpy as jnp
from jax import lax
from jax.sharding import PartitionSpec as P

CONV_CH = 2048
HEADS = 32
KV_HEADS = 8
HEAD_DIM = 64
WINDOW = 128


NORM_EPS = 1e-06
CHANNEL_EPS = 1e-05
ROPE_BASE = 10000.0


def sent_together(arrays, axis, dim, along):
    widths = [a.shape[along] for a in arrays]
    both = jnp.concatenate(arrays, axis=along)
    whole = lax.all_gather(both, axis, axis=dim, tiled=True)
    return tuple(jnp.split(whole, [sum(widths[:k]) for k in range(1, len(widths))], axis=along))


def shifted(value, axis, steps):
    count = lax.axis_size(axis)
    initial, last = (max(0, -steps), min(count, count - steps))
    return lax.ppermute(value, axis, [(source, source + steps) for source in range(initial, last)])


def from_everyone(shard, axis):
    peers = lax.axis_size(axis)
    return lax.all_to_all(
        jnp.broadcast_to(shard[None], (peers, *shard.shape)), axis, 0, 0, tiled=True
    )


def taken_together(shard, axis):
    everything = from_everyone(shard, axis)
    return jnp.sum(everything, axis=0)


def packed_total(arrays, axis):
    ravelled, at, finished = (jnp.concatenate([a.reshape(-1) for a in arrays]), 0, [])
    subtotal = taken_together(ravelled, axis)
    for a in arrays:
        finished.append(subtotal[at : at + a.size].reshape(a.shape))
        at += a.size
    return tuple(finished)


def turned_gather(arrays, axis, dims):
    turned = [jnp.moveaxis(a, dim, 0) for a, dim in zip(arrays, dims)]
    both = jnp.concatenate([t.reshape(len(t), -1) for t in turned], axis=1)
    whole, at, finished = (lax.all_gather(both, axis, axis=0, tiled=True), 0, [])
    for t, dim in zip(turned, dims):
        piece = whole[:, at : at + t[0].size].reshape(-1, *t.shape[1:])
        finished.append(jnp.moveaxis(piece, 0, dim))
        at += t[0].size
    return tuple(finished)


def cut_along(shard, dim, peers):
    dims = shard.shape
    pieces = shard.reshape(*dims[:dim], peers, dims[dim] // peers, *dims[dim + 1 :])
    return jnp.moveaxis(pieces, dim, 0)


def summed_on_arrival(shard, axis, dim):
    pieces = cut_along(shard, dim, lax.axis_size(axis))
    arrived = lax.all_to_all(pieces, axis, split_axis=0, concat_axis=0, tiled=True)
    return arrived.astype(jnp.float32).sum(axis=0)


def rotate(heads, positions):
    half_dim = heads.shape[-1] // 2
    inverse = ROPE_BASE ** (-jnp.arange(half_dim, dtype=jnp.float32) / half_dim)
    angles = positions.astype(jnp.float32)[:, None] * inverse[None, :]
    cosine = jnp.cos(angles)[:, None, :]
    sine = jnp.sin(angles)[:, None, :]
    as_float = heads.astype(jnp.float32)
    front_part = as_float[..., :half_dim]
    back_part = as_float[..., half_dim:]
    return jnp.concatenate(
        [front_part * cosine - back_part * sine, back_part * cosine + front_part * sine], axis=-1
    )


def shards(
    tokens,
    norm_gain,
    w_conv_value,
    w_conv_gate,
    w_query,
    w_key,
    w_value,
    conv_taps,
    ln_gain,
    sinks,
    out_conv,
    out_attn,
):
    as_float = tokens.astype(jnp.float32)
    normed = (
        as_float
        * lax.rsqrt(jnp.mean(as_float * as_float, axis=-1, keepdims=True) + NORM_EPS)
        * norm_gain.astype(jnp.float32)
    ).astype(jnp.bfloat16)
    row_count = normed.shape[0]
    pieces = sent_together((w_conv_value, w_conv_gate, w_query, w_key, w_value), "sp", 0, 1)
    projected = tuple(
        (jnp.dot(normed, piece, preferred_element_type=jnp.float32) for piece in pieces)
    )
    conv_value, conv_gate, query_raw, key_raw, value_rows = [
        item.astype(jnp.bfloat16) for item in projected
    ]
    glu = (conv_value.astype(jnp.float32) * jax.nn.sigmoid(conv_gate.astype(jnp.float32))).astype(
        jnp.bfloat16
    )
    offset = lax.axis_index("sp") * row_count
    positions = offset + jnp.arange(row_count, dtype=jnp.int32)
    query_heads = query_raw.shape[1] // HEAD_DIM
    key_heads = key_raw.shape[1] // HEAD_DIM
    query = rotate(query_raw.reshape(row_count, query_heads, HEAD_DIM), positions).astype(
        jnp.bfloat16
    )
    key = rotate(key_raw.reshape(row_count, key_heads, HEAD_DIM), positions).astype(jnp.bfloat16)
    reach = conv_taps.shape[0] - 1
    key_tail = key[row_count - WINDOW :]
    value_tail = value_rows.reshape(row_count, key_heads, HEAD_DIM)[row_count - WINDOW :]
    glu_tail = glu[row_count - reach :]
    glu_before = shifted(glu_tail, "sp", 1)
    key_before, value_before = shifted((key_tail, value_tail), "sp", 1)
    extended = jnp.concatenate([glu_before, glu], axis=0).astype(jnp.float32)
    conv_out = jnp.zeros((row_count, glu.shape[1]), jnp.float32)
    for tap in range(reach + 1):
        conv_out = conv_out + conv_taps[tap][None, :] * extended[tap : tap + row_count]
    sum_first = jnp.sum(conv_out, axis=-1)
    sum_second = jnp.sum(conv_out * conv_out, axis=-1)
    total_first, total_second = packed_total((sum_first, sum_second), "tp")
    mean = (total_first / CONV_CH)[:, None]
    var = (total_second / CONV_CH)[:, None] - mean * mean
    conv_branch = jax.nn.silu(
        (conv_out - mean) * lax.rsqrt(var + CHANNEL_EPS) * ln_gain[None, :]
    ).astype(jnp.bfloat16)
    group = HEADS // KV_HEADS
    blocks = row_count // WINDOW
    q_blocks = query.reshape(blocks, WINDOW, key_heads, group, HEAD_DIM)
    key_blocks = jnp.concatenate([key_before, key], axis=0).reshape(
        blocks + 1, WINDOW, key_heads, HEAD_DIM
    )
    value_all = jnp.concatenate(
        [value_before, value_rows.reshape(row_count, key_heads, HEAD_DIM)], axis=0
    )
    value_blocks = value_all.reshape(blocks + 1, WINDOW, key_heads, HEAD_DIM)
    key_window = jnp.concatenate([key_blocks[:-1], key_blocks[1:]], axis=1)
    value_window = jnp.concatenate([value_blocks[:-1], value_blocks[1:]], axis=1)
    scores = jnp.einsum(
        "nqhgd,nkhd->nhgqk", q_blocks, key_window, preferred_element_type=jnp.float32
    ) * HEAD_DIM ** (-0.5)
    query_index = jnp.arange(WINDOW)[:, None] + WINDOW
    key_index = jnp.arange(2 * WINDOW)[None, :]
    band = (key_index <= query_index) & (query_index - key_index < WINDOW)
    block_index = jnp.arange(blocks)[:, None, None]
    allowed = band[None] & (offset + block_index * WINDOW + key_index[None] - WINDOW >= 0)
    allowed = allowed[:, None, None]
    totals = jnp.sum(jnp.where(allowed, jnp.exp(scores), 0.0), axis=-1)
    totals = totals + jnp.exp(sinks).reshape(1, key_heads, group, 1)
    log_total = jnp.log(totals)
    weights = jnp.where(allowed, jnp.exp(scores - log_total[..., None]), 0.0).astype(jnp.bfloat16)
    attended = jnp.einsum(
        "nhgqk,nkhd->nqhgd", weights, value_window, preferred_element_type=jnp.float32
    )
    attn_branch = attended.astype(jnp.bfloat16).reshape(row_count, query_heads * HEAD_DIM)
    log_sums = log_total.transpose(1, 2, 0, 3).reshape(query_heads, row_count)
    cols_conv, cols_attn = turned_gather((out_conv, out_attn), "sp", (1, 1))
    mixed = summed_on_arrival(
        (
            jnp.dot(conv_branch, cols_conv, preferred_element_type=jnp.float32)
            + jnp.dot(attn_branch, cols_attn, preferred_element_type=jnp.float32)
        ).astype(jnp.bfloat16),
        "tp",
        0,
    )
    return (mixed.astype(jnp.bfloat16), log_sums)


def solution(mesh):
    in_specs = (
        P("sp", None),
        P(),
        P("sp", "tp"),
        P("sp", "tp"),
        P("sp", "tp"),
        P("sp", "tp"),
        P("sp", "tp"),
        P(None, "tp"),
        P("tp"),
        P("tp"),
        P("tp", "sp"),
        P("tp", "sp"),
    )
    out_specs = (P(("sp", "tp"), None), P("tp", "sp"))
    return jax.shard_map(shards, mesh=mesh, in_specs=in_specs, out_specs=out_specs, check_vma=False)
```

profile of v0, /device:TPU:1, one launch (start us, length us, event | category | flops | bytes accessed | tf_op | source)
XLA Modules:
  0.0 231.2 jit_solution(13513248119261540660)
XLA Ops:
  7.2 0.9 constant_dynamic-update-slice_fusion.4
  8.1 0.7 constant_dynamic-update-slice_fusion.3
  8.8 0.7 constant_dynamic-update-slice_fusion.2
  9.5 0.7 constant_dynamic-update-slice_fusion.1
  10.2 0.7 constant_dynamic-update-slice_fusion
  10.9 0.6 copy-done.2
  11.6 1.3 pad_maximum_fusion.4
  13.0 0.7 convert_element_type.78
  13.7 0.7 exp.19
  15.1 2.1 fusion
  17.2 1.0 fusion.126
  18.2 1.7 fusion.125
  20.5 84.2 %all-gather.3.cloned.1.call-done = bf16[2048,1792]{1,0:T(8,128)(2,1)} async-done(((bf16[16,1792]{1,0:T(8,128)(2,1)}), bf16[2048,1792]{1,0:T(8,128)(2,1)}) %all-gather.3.cloned.1.call-update) | async-done | bytes 7340048 | tf_op jit(solution)/shard_map/all_gather | solution.py:21
  104.7 2.6 %convolution_convert_fusion.1 = bf16[512,128]{0,1:T(8,128)(2,1)S(1)} fusion(bf16[2048,1792]{1,0:T(8,128)(2,1)} %all-gather.3.cloned.1.call-done, bf16[512,2048]{1,0:T(8,128)(2,1)} %param.12, f32[2048]{0:T(1024)S(1)} %convert_element_type.78, f32[512]{0:T(512)S(1)} %add_rsqrt_fusion.1), kind=kOutput, calls=%fused_computation.41 | convolution fusion | flops 272695296 | bytes 2762752 | tf_op jit(solution)/shard_map/dot_general | solution.py:112
  107.4 2.1 convolution_convert_fusion
  109.6 3.0 %collective-permute-start.2 = (bf16[128,2,64]{0,2,1:T(8,128)(2,1)S(1)}, bf16[128,2,64]{0,2,1:T(8,128)(2,1)S(1)}, u32[]{:S(2)}, u32[]{:S(2)}) collective-permute-start(bf16[128,2,64]{0,2,1:T(8,128)(2,1)S(1)} %pad_maximum_fusion.3), channel_id=1, source_target_pairs={{0,4},{4,8},{8,12},{12,16},{16,20},{20,24},{24,28},{28,32},{32,36}... | collective-permute-start | bytes 98312 | tf_op jit(solution)/shard_map/ppermute | solution.py:28
  112.6 3.0 %fusion.47 = bf16[512,512]{0,1:T(8,128)(2,1)S(1)} fusion(bf16[2048,1792]{1,0:T(8,128)(2,1)} %all-gather.3.cloned.1.call-done, bf16[512,2048]{1,0:T(8,128)(2,1)S(1)} %copy-done, f32[2048]{0:T(1024)S(1)} %convert_element_type.78, f32[512]{0:T(512)S(1)} %add_rsqrt_fusion.1), kind=kOutput, calls=%fused_computation.35 | convolution fusion | flops 1078198272 | bytes 4728832 | tf_op jit(solution)/shard_map/dot_general | solution.py:112
  115.7 1.5 fusion.56
  117.2 1.3 fusion.50
  118.5 2.1 collective-permute-start
  121.1 3.7 %collective-permute-start.1 = (bf16[128,2,64]{0,2,1:T(8,128)(2,1)S(1)}, bf16[128,2,64]{0,2,1:T(8,128)(2,1)S(1)}, u32[]{:S(2)}, u32[]{:S(2)}) collective-permute-start(bf16[128,2,64]{0,2,1:T(8,128)(2,1)S(1)} %bitcast.113), channel_id=1, source_target_pairs={{0,4},{4,8},{8,12},{12,16},{16,20},{20,24},{24,28},{28,32},{32,36}... | collective-permute-start | bytes 98312 | tf_op jit(solution)/shard_map/ppermute | solution.py:28
  125.1 5.1 %fusion.123 = (f32[512]{0:T(512)S(1)}, f32[512]{0:T(512)S(1)}, f32[512,512]{1,0:T(8,128)S(1)}) fusion(f32[542,512]{1,0:T(8,128)S(1)} %maximum_convert_fusion, f32[512]{0:T(512)S(1)} %bitcast.127, f32[512]{0:T(512)S(1)} %bitcast.128, f32[512]{0:T(512)S(1)} %bitcast.130, f32[512]{0:T(512)S(1)} %bitcast.131, f32[512]{0:T(512)S(1)} %bitcast.132, ...), kind=kLoop, calls=%fused_computation.167 | loop fusion | flops 16776192 | bytes 33622016 | tf_op jit(solution)/shard_map/reduce_sum | solution.py:138
  130.2 0.6 broadcast_in_dim.14
  130.8 4.0 %all-to-all-start = ((f32[4,1,1024]{2,1,0:T(1,128)}), f32[4,1,1024]{2,1,0:T(1,128)S(1)}, u32[]{:S(2)}, u32[]{:S(2)}) async-start(f32[4,1,1024]{2,1,0:T(1,128)} %broadcast_in_dim.14), calls=%async_computation | async-start | bytes 32768 | tf_op jit(solution)/shard_map/all_to_all | solution.py:33
  134.8 1.1 fusion.4
  136.1 0.9 fusion.59
  137.4 1.6 all-to-all-done
  139.0 49.8 %all-gather.5.cloned.1.call-done = bf16[2048,1024]{1,0:T(8,128)(2,1)} async-done(((bf16[16,1024]{1,0:T(8,128)(2,1)}), bf16[2048,1024]{1,0:T(8,128)(2,1)}) %all-gather.5.cloned.1.call-update) | async-done | bytes 4194320 | tf_op jit(solution)/shard_map/all_gather | solution.py:55
  188.9 3.2 %fusion.13 = f32[512,2048]{1,0:T(8,128)S(1)} fusion(bf16[2048,1024]{1,0:T(8,128)(2,1)} %all-gather.5.cloned.1.call-done, f32[512,512]{1,0:T(8,128)S(1)} %get-tuple-element.4, f32[512]{0:T(512)S(1)} %copy-done.8, f32[512]{0:T(512)S(1)} %get-tuple-element.41, f32[512]{0:T(512)S(1)} %get-tuple-element.40), kind=kOutput, calls=%fused_computation.17 | convolution fusion | flops 1075838976 | bytes 7346176 | tf_op jit(solution)/shard_map/dot_general | solution.py:179
  192.1 1.3 add_convert_fusion
  193.4 29.6 %all_to_all.11 = bf16[4,128,2048]{2,1,0:T(8,128)(2,1)S(1)} all-to-all(bf16[4,128,2048]{2,1,0:T(8,128)(2,1)S(1)} %bitcast.108), channel_id=1, replica_groups=mesh['sp'=128,'tp'=4] {'tp'}, dimensions={0} | all-to-all | bytes 4194304 | tf_op jit(solution)/shard_map/all_to_all | solution.py:71
  223.0 1.3 reduce_sum.62
  (61 shorter events, 2.8 us)
Async XLA Ops:
  7.2 100.2 %copy-start = (bf16[512,2048]{1,0:T(8,128)(2,1)S(1)}, bf16[512,2048]{1,0:T(8,128)(2,1)}, u32[]{:S(2)}) copy-start(bf16[512,2048]{1,0:T(8,128)(2,1)} %param.12) | copy-start | bytes 6291460
  7.2 97.5 %all-gather.3.cloned.1.call-start = ((), (), s32[]{:S(2)}) async-start(), calls=%async_computation.2 | async-start | bytes 7397376 | tf_op jit(solution)/shard_map/all_gather | solution.py:21
  10.9 0.6 copy-start.2
  11.6 177.3 %all-gather.5.cloned.1.call-start = ((), (), s32[]{:S(2)}) async-start(), calls=%async_computation.3 | async-start | bytes 4227072 | tf_op jit(solution)/shard_map/all_gather | solution.py:55
  107.3 8.3 %slice-start = ((s8[7340032]{0:T(1024)(128)(4,1)}), s8[4194304]{0:T(1024)(128)(4,1)S(1)}, s32[]{:S(2)}) async-start(s8[7340032]{0:T(1024)(128)(4,1)} %bitcast.148), calls=%async_computation.4 | async-start | bytes 8388608
  109.5 6.1 %slice-start.1 = ((s8[7340032]{0:T(1024)(128)(4,1)}), s8[3145728]{0:T(1024)(128)(4,1)S(1)}, s32[]{:S(2)}) async-start(s8[7340032]{0:T(1024)(128)(4,1)} %bitcast.148), calls=%async_computation.5 | async-start | bytes 6291456
  109.6 25.2 %collective-permute-start.2 = (bf16[128,2,64]{0,2,1:T(8,128)(2,1)S(1)}, bf16[128,2,64]{0,2,1:T(8,128)(2,1)S(1)}, u32[]{:S(2)}, u32[]{:S(2)}) collective-permute-start(bf16[128,2,64]{0,2,1:T(8,128)(2,1)S(1)} %pad_maximum_fusion.3), channel_id=1, source_target_pairs={{0,4},{4,8},{8,12},{12,16},{16,20},{20,24},{24,28},{28,32},{32,36}... | collective-permute-start | bytes 98312 | tf_op jit(solution)/shard_map/ppermute | solution.py:28
  118.5 6.6 %copy-start.4 = (f32[1,512]{1,0:T(1,128)S(1)}, f32[1,512]{1,0:T(1,128)}, u32[]{:S(2)}) copy-start(f32[1,512]{1,0:T(1,128)} %get-tuple-element.25) | copy-start | bytes 6148
  118.5 6.6 %copy-start.5 = (f32[1,512]{1,0:T(1,128)S(1)}, f32[1,512]{1,0:T(1,128)}, u32[]{:S(2)}) copy-start(f32[1,512]{1,0:T(1,128)} %get-tuple-element.26) | copy-start | bytes 6148
  118.5 6.6 %copy-start.6 = (f32[1,512]{1,0:T(1,128)S(1)}, f32[1,512]{1,0:T(1,128)}, u32[]{:S(2)}) copy-start(f32[1,512]{1,0:T(1,128)} %get-tuple-element.27) | copy-start | bytes 6148
  118.5 6.3 %collective-permute-start = (bf16[30,512]{1,0:T(8,128)(2,1)S(1)}, bf16[30,512]{1,0:T(8,128)(2,1)S(1)}, u32[]{:S(2)}, u32[]{:S(2)}) collective-permute-start(bf16[30,512]{1,0:T(8,128)(2,1)S(1)} %slice.319), channel_id=1, source_target_pairs={{0,4},{4,8},{8,12},{12,16},{16,20},{20,24},{24,28},{28,32},{32,36}... | collective-permute-start | bytes 92168 | tf_op jit(solution)/shard_map/ppermute | solution.py:28
  121.1 13.7 %collective-permute-start.1 = (bf16[128,2,64]{0,2,1:T(8,128)(2,1)S(1)}, bf16[128,2,64]{0,2,1:T(8,128)(2,1)S(1)}, u32[]{:S(2)}, u32[]{:S(2)}) collective-permute-start(bf16[128,2,64]{0,2,1:T(8,128)(2,1)S(1)} %bitcast.113), channel_id=1, source_target_pairs={{0,4},{4,8},{8,12},{12,16},{16,20},{20,24},{24,28},{28,32},{32,36}... | collective-permute-start | bytes 98312 | tf_op jit(solution)/shard_map/ppermute | solution.py:28
  130.2 5.8 %copy-start.7 = (f32[2,4]{1,0:T(2,128)S(1)}, f32[2,4]{1,0:T(2,128)}, u32[]{:S(2)}) copy-start(f32[2,4]{1,0:T(2,128)} %add.243) | copy-start | bytes 100
  130.8 8.2 %all-to-all-start = ((f32[4,1,1024]{2,1,0:T(1,128)}), f32[4,1,1024]{2,1,0:T(1,128)S(1)}, u32[]{:S(2)}, u32[]{:S(2)}) async-start(f32[4,1,1024]{2,1,0:T(1,128)} %broadcast_in_dim.14), calls=%async_computation | async-start | bytes 32768 | tf_op jit(solution)/shard_map/all_to_all | solution.py:33
  135.9 52.9 %copy-start.8 = (f32[512]{0:T(512)S(1)}, f32[512]{0:T(512)}, u32[]{:S(2)}) copy-start(f32[512]{0:T(512)} %param.20) | copy-start | bytes 6148
  136.1 56.0 %copy-start.3 = (f32[4,2,4,128]{3,2,1,0:T(4,128)}, f32[4,2,4,128]{3,2,1,0:T(4,128)S(1)}, u32[]{:S(2)}) copy-start(f32[4,2,4,128]{3,2,1,0:T(4,128)S(1)} %add_log_fusion) | copy-start | bytes 49156
  188.9 3.2 %copy-start.1 = (bf16[2048,1024]{1,0:T(8,128)(2,1)S(1)}, bf16[2048,1024]{1,0:T(8,128)(2,1)}, u32[]{:S(2)}) copy-start(bf16[2048,1024]{1,0:T(8,128)(2,1)} %all-gather.5.cloned.1.call-done) | copy-start | bytes 12582916
Sparse Core Ops, SparseCore 0:
  11.7 92.9 all-gather.2
  107.8 80.9 all-gather.4
where the time goes:
time: 232 us; the launch traced here: 231 us
  waiting for transfers between devices  136 us (59%)
  blocking collectives  29.6 us (13%)
  matrix products  16.9 us (7%)
  between operations  14.5 us (6%)
  starting transfers between devices  12.9 us (6%)
  other arithmetic  11.8 us (5%)
  local copies, waits for them, and re-layouts  9.71 us (4%)
    all_gather x1, waiting for transfers between devices, sent_together(): whole = lax.all_gather(both, axis, axis=dim, tiled=True)  84.2 us
    all_gather x1, waiting for transfers between devices, turned_gather(): lax.all_gather(both, axis, axis=0, tiled=True)  49.8 us
    all_to_all x1, blocking collectives, summed_on_arrival(): lax.all_to_all(pieces, axis, split_axis=0, concat_axis=0, tiled=True)  29.6 us
    dot_general x5, matrix products, shards(): jnp.dot(normed, piece, preferred_element_type=jnp.float32)  10.4 us
    ppermute x3, starting transfers between devices, shifted(): lax.ppermute(value, axis, [(source, source + steps) for source in range(i...  8.87 us
    reduce_sum x1, other arithmetic, shards(): sum_first = jnp.sum(conv_out, axis=-1)  5.05 us
  transfers between devices with their start and end apart: 6, of which 3 were waited for; matrix products, arithmetic and copies ran while one was open for 12% of the time, Pallas kernels for 0%

commit v1 on v0

--- a/solution.py
+++ b/solution.py
@@ -1,6 +1,8 @@
 import jax
 import jax.numpy as jnp
 from jax import lax
+from jax.experimental import pallas as pl
+from jax.experimental.pallas import tpu as pltpu
 from jax.sharding import PartitionSpec as P
 
 CONV_CH = 2048
@@ -13,6 +15,151 @@
 NORM_EPS = 1e-06
 CHANNEL_EPS = 1e-05
 ROPE_BASE = 10000.0
+MESH = pl.DeviceIdType.MESH
+
+NY = 8
+NZ = 8
+WIN_COLS = 1792
+WOUT_COLS = 1024
+LAG = 4
+RELS = (-3, -2, -1, 0, 1, 2, 3, 4)
+
+
+def hops(first, a, b):
+    main, side = (a, b) if first == 0 else (b, a)
+    onward = []
+    if side == 0:
+        if 0 <= main < 4:
+            onward.append((first, 1, main + 1, 0))
+        if -3 < main <= 0:
+            onward.append((first, -1, main - 1, 0))
+    if 0 <= side < 4:
+        onward.append((1 - first, 1, main, side + 1))
+    if -3 < side <= 0:
+        onward.append((1 - first, -1, main, side - 1))
+    return [
+        (axis, sign, m, s) if first == 0 else (axis, sign, s, m)
+        for axis, sign, m, s in onward
+    ]
+
+
+def pieces_at(distance):
+    found = [(a, b) for a in RELS for b in RELS if abs(a) + abs(b) == distance]
+    return sorted(found, key=lambda ab: (min(abs(ab[0]), abs(ab[1])), ab))
+
+
+def gather_kernel(win_ref, wout_ref, gin, gout, *sems):
+    me = lax.axis_index("sp")
+    core = lax.rem(me, 2)
+    y = lax.rem(me // 2, NY)
+    z = me // (2 * NY)
+    ahead = 1 - 2 * core
+
+    def device(zz, yy, cc):
+        return {"sp": (zz * NY + yy) * 2 + cc}
+
+    def near(axis, sign):
+        step = sign * ahead
+        if axis == 0:
+            return device(lax.rem(z + step + NZ, NZ), y, core)
+        return device(z, lax.rem(y + step + NY, NY), core)
+
+    partner = device(z, y, 1 - core)
+    neighbours = [near(0, 1), near(0, -1), near(1, 1), near(1, -1), partner]
+    barrier = pltpu.get_barrier_semaphore()
+    for one in neighbours:
+        pl.semaphore_signal(barrier, inc=1, device_id=one, device_id_type=MESH)
+    pl.semaphore_wait(barrier, len(neighbours))
+
+    started = []
+
+    def stage(own, full, recv, send, precv, psend, distance):
+        cols = full.shape[-1] // 2
+        for a, b in pieces_at(distance):
+            oz = lax.rem(z - a * ahead + NZ, NZ)
+            oy = lax.rem(y - b * ahead + NY, NY)
+            slot = full.at[oz, oy, core]
+            for first in range(2):
+                part = (slice(None), pl.ds(first * cols, cols))
+                source = own.at[part] if distance == 0 else slot.at[part]
+                target = slot.at[part]
+                if distance > 0:
+                    pltpu.make_async_remote_copy(
+                        src_ref=target,
+                        dst_ref=target,
+                        send_sem=send.at[first, 0, a + 3, b + 3],
+                        recv_sem=recv.at[first, a + 3, b + 3],
+                        device_id=near(0, 1),
+                        device_id_type=MESH,
+                    ).wait_recv()
+                for way, (axis, sign, a2, b2) in enumerate(hops(first, a, b)):
+                    copy = pltpu.make_async_remote_copy(
+                        src_ref=source,
+                        dst_ref=target,
+                        send_sem=send.at[first, way, a + 3, b + 3],
+                        recv_sem=recv.at[first, a2 + 3, b2 + 3],
+                        device_id=near(axis, sign),
+                        device_id_type=MESH,
+                    )
+                    copy.start()
+                    started.append(copy)
+            copy = pltpu.make_async_remote_copy(
+                src_ref=own if distance == 0 else slot,
+                dst_ref=slot,
+                send_sem=psend.at[a + 3, b + 3],
+                recv_sem=precv.at[a + 3, b + 3],
+                device_id=partner,
+                device_id_type=MESH,
+            )
+            copy.start()
+            started.append(copy)
+
+    def from_partner(full, precv, psend):
+        for a in RELS:
+            for b in RELS:
+                oz = lax.rem(z + a * ahead + NZ, NZ)
+                oy = lax.rem(y + b * ahead + NY, NY)
+                slot = full.at[oz, oy, 1 - core]
+                pltpu.make_async_remote_copy(
+                    src_ref=slot,
+                    dst_ref=slot,
+                    send_sem=psend.at[a + 3, b + 3],
+                    recv_sem=precv.at[a + 3, b + 3],
+                    device_id=partner,
+                    device_id_type=MESH,
+                ).wait_recv()
+
+    for tick in range(9 + LAG):
+        if tick < 9:
+            stage(win_ref, gin, *sems[:4], tick)
+        if tick == 0:
+            gin[z, y, core] = win_ref[...]
+            gout[z, y, core] = wout_ref[...]
+        if tick >= LAG:
+            stage(wout_ref, gout, *sems[4:], tick - LAG)
+    from_partner(gin, *sems[2:4])
+    from_partner(gout, *sems[6:8])
+    for copy in started:
+        copy.wait_send()
+
+
+def gathered(win, wout):
+    dma = pltpu.SemaphoreType.DMA
+    one = [dma((2, 8, 8)), dma((2, 4, 8, 8)), dma((8, 8)), dma((8, 8))]
+    vmem = pl.BlockSpec(memory_space=pltpu.VMEM)
+    gin, gout = pl.pallas_call(
+        gather_kernel,
+        out_shape=(
+            jax.ShapeDtypeStruct((NZ, NY, 2, 16, WIN_COLS), jnp.bfloat16),
+            jax.ShapeDtypeStruct((NZ, NY, 2, 16, WOUT_COLS), jnp.bfloat16),
+        ),
+        in_specs=[vmem, vmem],
+        out_specs=(vmem, vmem),
+        scratch_shapes=one + one,
+        compiler_params=pltpu.CompilerParams(collective_id=0, has_side_effects=True),
+        name="gather_weights",
+    )(win, wout)
+    return gin.reshape(2048, WIN_COLS), gout.reshape(2048, WOUT_COLS)
 
 
 def sent_together(arrays, axis, dim, along):
@@ -107,7 +254,11 @@
         * norm_gain.astype(jnp.float32)
     ).astype(jnp.bfloat16)
     row_count = normed.shape[0]
-    pieces = sent_together((w_conv_value, w_conv_gate, w_query, w_key, w_value), "sp", 0, 1)
+    win, wout = gathered(
+        jnp.concatenate([w_conv_value, w_conv_gate, w_query, w_key, w_value], axis=1),
+        jnp.concatenate([out_conv.T, out_attn.T], axis=1),
+    )
+    pieces = jnp.split(win, (512, 1024, 1536, 1664), axis=1)
     projected = tuple(
         (jnp.dot(normed, piece, preferred_element_type=jnp.float32) for piece in pieces)
     )
@@ -173,11 +324,10 @@
     )
     attn_branch = attended.astype(jnp.bfloat16).reshape(row_count, query_heads * HEAD_DIM)
     log_sums = log_total.transpose(1, 2, 0, 3).reshape(query_heads, row_count)
-    cols_conv, cols_attn = turned_gather((out_conv, out_attn), "sp", (1, 1))
     mixed = summed_on_arrival(
         (
-            jnp.dot(conv_branch, cols_conv, preferred_element_type=jnp.float32)
-            + jnp.dot(attn_branch, cols_attn, preferred_element_type=jnp.float32)
+            jnp.dot(conv_branch, wout[:, :512].T, preferred_element_type=jnp.float32)
+            + jnp.dot(attn_branch, wout[:, 512:].T, preferred_element_type=jnp.float32)
         ).astype(jnp.bfloat16),
         "tp",
         0,

time: 232 us -> 162 us (0.70)
  waiting for transfers between devices: 136 us -> 1.61 us
  Pallas kernels: 0 us -> 84.5 us
  between operations: 14.5 us -> 1.09 us
  local copies, waits for them, and re-layouts: 9.71 us -> 5.68 us
  blocking collectives: 29.6 us -> 27.1 us
  starting transfers between devices: 12.9 us -> 10.5 us
    all_gather x2 -> x0, waiting for transfers between devices: 134 us -> none  [the longest x1 84.2 us: sent_together(): whole = lax.all_gather(both, axis, axis=dim, tiled=True)]
    pallas_call x0 -> x1, Pallas kernels: none -> 84.5 us  [gathered(): pl.pallas_call(gather_kernel, out_shape=(jax.ShapeDtypeStruct((NZ, NY, 2,...]
    slice x2, local copies, waits for them, and re-layouts: 2.76 us -> 0.05 us  [shards(): conv_taps[tap][None, :] * extended[tap:tap + row_count]]
    all_to_all x1, blocking collectives: 29.6 us -> 27.1 us  [summed_on_arrival(): lax.all_to_all(pieces, axis, split_axis=0, concat_axis=0, tiled=True)]
    ppermute x3, starting transfers between devices: 8.87 us -> 6.47 us  [shifted(): lax.ppermute(value, axis, [(source, source + steps) for source in range(i...]
  transfers between devices with their start and end apart: 6 -> 4, of which waited for: 3 -> 1; matrix products, arithmetic and copies ran while one was open for 12% -> 11% of each run, Pallas kernels for 0% -> 0%
where the time goes in v1:
time: 162 us; the launch traced here: 159 us
  Pallas kernels  84.5 us (52%)
  blocking collectives  27.1 us (17%)
  matrix products  16.9 us (10%)
  other arithmetic  11.9 us (7%)
  starting transfers between devices  10.5 us (6%)
  local copies, waits for them, and re-layouts  5.68 us (4%)
    pallas_call x1, Pallas kernels, gathered(): pl.pallas_call(gather_kernel, out_shape=(jax.ShapeDtypeStruct((NZ, NY, 2,...  84.5 us
    all_to_all x1, blocking collectives, summed_on_arrival(): lax.all_to_all(pieces, axis, split_axis=0, concat_axis=0, tiled=True)  27.1 us
    dot_general x5, matrix products, shards(): jnp.dot(normed, piece, preferred_element_type=jnp.float32)  10.4 us
    ppermute x3, starting transfers between devices, shifted(): lax.ppermute(value, axis, [(source, source + steps) for source in range(i...  6.47 us
    reduce_sum x1, other arithmetic, shards(): sum_first = jnp.sum(conv_out, axis=-1)  5.05 us
    all_to_all x1, starting transfers between devices, from_everyone(): lax.all_to_all(jnp.broadcast_to(shard[None], (peers, *shard.shape)), axis...  4.02 us
    unnamed x22, local copies, waits for them, and re-layouts  3.52 us
  transfers between devices with their start and end apart: 4, of which 1 were waited for; matrix products, arithmetic and copies ran while one was open for 11% of the time, Pallas kernels for 0%

profile of v1, /device:TPU:1, one launch (start us, length us, event | category | flops | bytes accessed | tf_op | source)
XLA Modules:
  0.0 159.3 jit_solution(1610114801133944275)
XLA Ops:
  0.6 2.2 %fusion = f32[512]{0:T(512)S(1)} fusion(bf16[512,2048]{1,0:T(8,128)(2,1)} %param.12), kind=kLoop, calls=%fused_computation.2 | loop fusion | flops 3145216 | bytes 2099200 | tf_op jit(solution)/shard_map/reduce_sum | solution.py:253
  2.9 0.7 convert_element_type.78
  3.6 0.7 constant_dynamic-update-slice_fusion.4
  4.3 1.3 pad_maximum_fusion.4.wout_ref
  5.6 0.7 constant_dynamic-update-slice_fusion.3
  6.4 0.7 constant_dynamic-update-slice_fusion.2
  7.1 0.7 constant_dynamic-update-slice_fusion.1
  7.8 0.7 constant_dynamic-update-slice_fusion.win_ref
  8.5 0.6 copy-done.2
  9.1 84.5 %gather_weights.1 = (bf16[8,8,2,16,1792]{4,3,2,1,0:T(8,128)(2,1)}, bf16[8,8,2,16,1024]{4,3,2,1,0:T(8,128)(2,1)}) custom-call(bf16[16,1792]{1,0:T(8,128)(2,1)} %copy-done.2, bf16[16,1024]{1,0:T(8,128)(2,1)} %pad_maximum_fusion.4.wout_ref), custom_call_target="tpu_custom_call" | custom-call | tf_op jit(solution)/shard_map/gather_weights/pallas_call | solution.py:150
  93.6 2.6 %convolution_convert_fusion.1 = bf16[512,128]{0,1:T(8,128)(2,1)S(1)} fusion(bf16[2048,1792]{1,0:T(8,128)(2,1)} %bitcast.152, bf16[512,2048]{1,0:T(8,128)(2,1)} %param.12, f32[2048]{0:T(1024)S(1)} %convert_element_type.78, f32[512]{0:T(512)S(1)} %add_rsqrt_fusion.1), kind=kOutput, calls=%fused_computation.41 | convolution fusion | flops 272695296 | bytes 2762752 | tf_op jit(solution)/shard_map/dot_general | solution.py:263
  96.2 1.9 %collective-permute-start.1 = (bf16[128,2,64]{0,2,1:T(8,128)(2,1)S(1)}, bf16[128,2,64]{0,2,1:T(8,128)(2,1)S(1)}, u32[]{:S(2)}, u32[]{:S(2)}) collective-permute-start(bf16[128,2,64]{0,2,1:T(8,128)(2,1)S(1)} %bitcast.117), channel_id=1, source_target_pairs={{0,4},{4,8},{8,12},{12,16},{16,20},{20,24},{24,28},{28,32},{32,36}... | collective-permute-start | bytes 98312 | tf_op jit(solution)/shard_map/ppermute | solution.py:175
  98.2 1.9 %convolution_convert_fusion = bf16[512,128]{0,1:T(8,128)(2,1)S(1)} fusion(bf16[2048,1792]{1,0:T(8,128)(2,1)} %bitcast.153, bf16[512,2048]{1,0:T(8,128)(2,1)S(1)} %copy-done, f32[2048]{0:T(1024)S(1)} %convert_element_type.78, f32[512]{0:T(512)S(1)} %add_rsqrt_fusion.1), kind=kOutput, calls=%fused_computation.40 | convolution fusion | flops 272695296 | bytes 2762752 | tf_op jit(solution)/shard_map/dot_general | solution.py:263
  100.2 0.3 multiply_cosine_fusion
  100.6 2.3 %collective-permute-start.2 = (bf16[128,2,64]{0,2,1:T(8,128)(2,1)S(1)}, bf16[128,2,64]{0,2,1:T(8,128)(2,1)S(1)}, u32[]{:S(2)}, u32[]{:S(2)}) collective-permute-start(bf16[128,2,64]{0,2,1:T(8,128)(2,1)S(1)} %pad_maximum_fusion.3), channel_id=1, source_target_pairs={{0,4},{4,8},{8,12},{12,16},{16,20},{20,24},{24,28},{28,32},{32,36}... | collective-permute-start | bytes 98312 | tf_op jit(solution)/shard_map/ppermute | solution.py:175
  102.9 3.0 %fusion.56 = f32[512,512]{1,0:T(8,128)S(1)} fusion(bf16[2048,1792]{1,0:T(8,128)(2,1)} %bitcast.154, bf16[512,2048]{1,0:T(8,128)(2,1)S(1)} %copy-done, f32[2048]{0:T(1024)S(1)} %convert_element_type.78, f32[512]{0:T(512)S(1)} %add_rsqrt_fusion.1), kind=kOutput, calls=%fused_computation.38 | convolution fusion | flops 1079246848 | bytes 5253120 | tf_op jit(solution)/shard_map/dot_general | solution.py:263
  106.0 1.4 fusion.50
  107.3 2.2 %collective-permute-start = (bf16[30,512]{1,0:T(8,128)(2,1)S(1)}, bf16[30,512]{1,0:T(8,128)(2,1)S(1)}, u32[]{:S(2)}, u32[]{:S(2)}) collective-permute-start(bf16[30,512]{1,0:T(8,128)(2,1)S(1)} %slice.319), channel_id=1, source_target_pairs={{0,4},{4,8},{8,12},{12,16},{16,20},{20,24},{24,28},{28,32},{32,36}... | collective-permute-start | bytes 92168 | tf_op jit(solution)/shard_map/ppermute | solution.py:175
  109.7 1.4 fusion.47
  111.4 0.2 subtract_convert_fusion
  111.6 0.2 broadcast_and_fusion
  112.4 5.1 %fusion.123 = (f32[512]{0:T(512)S(1)}, f32[512]{0:T(512)S(1)}, f32[512,512]{1,0:T(8,128)S(1)}) fusion(f32[542,512]{1,0:T(8,128)S(1)} %maximum_convert_fusion, f32[512]{0:T(512)S(1)} %bitcast.150, f32[512]{0:T(512)S(1)} %bitcast.151, f32[512]{0:T(512)S(1)} %bitcast.122, f32[512]{0:T(512)S(1)} %bitcast.123, f32[512]{0:T(512)S(1)} %bitcast.124, ...), kind=kLoop, calls=%fused_computation.167 | loop fusion | flops 16776192 | bytes 33622016 | tf_op jit(solution)/shard_map/reduce_sum | solution.py:289
  117.5 0.6 broadcast_in_dim.14
  118.1 4.0 %all-to-all-start = ((f32[4,1,1024]{2,1,0:T(1,128)}), f32[4,1,1024]{2,1,0:T(1,128)S(1)}, u32[]{:S(2)}, u32[]{:S(2)}) async-start(f32[4,1,1024]{2,1,0:T(1,128)} %broadcast_in_dim.14), calls=%async_computation | async-start | bytes 32768 | tf_op jit(solution)/shard_map/all_to_all | solution.py:180
  122.1 1.1 fusion.4
  123.4 0.9 fusion.59
  124.3 0.4 copy.46
  124.7 1.6 %all-to-all-done = f32[4,1,1024]{2,1,0:T(1,128)S(1)} async-done(((f32[4,1,1024]{2,1,0:T(1,128)}), f32[4,1,1024]{2,1,0:T(1,128)S(1)}, u32[]{:S(2)}, u32[]{:S(2)}) %all-to-all-start) | async-done | bytes 16416 | tf_op jit(solution)/shard_map/all_to_all | solution.py:180
  126.4 3.2 %fusion.13 = f32[512,2048]{1,0:T(8,128)S(1)} fusion(bf16[2048,1024]{1,0:T(8,128)(2,1)} %bitcast.112, f32[512,512]{1,0:T(8,128)S(1)} %get-tuple-element.8, f32[512]{0:T(512)S(1)} %copy-done.5, f32[512]{0:T(512)S(1)} %get-tuple-element.45, f32[512]{0:T(512)S(1)} %get-tuple-element.44), kind=kOutput, calls=%fused_computation.17 | convolution fusion | flops 1075838976 | bytes 7346176 | tf_op jit(solution)/shard_map/dot_general | solution.py:329
  129.6 1.3 add_convert_fusion
  130.9 27.1 %all_to_all.11 = bf16[4,128,2048]{2,1,0:T(8,128)(2,1)S(1)} all-to-all(bf16[4,128,2048]{2,1,0:T(8,128)(2,1)S(1)} %bitcast.110), channel_id=1, replica_groups=mesh['sp'=128,'tp'=4] {'tp'}, dimensions={0} | all-to-all | bytes 4194304 | tf_op jit(solution)/shard_map/all_to_all | solution.py:218
  158.0 1.3 reduce_sum.62
  (52 shorter events, 1.2 us)
Async XLA Ops:
  0.6 97.5 %copy-start = (bf16[512,2048]{1,0:T(8,128)(2,1)S(1)}, bf16[512,2048]{1,0:T(8,128)(2,1)}, u32[]{:S(2)}) copy-start(bf16[512,2048]{1,0:T(8,128)(2,1)} %param.12) | copy-start | bytes 6291460
  8.5 0.6 copy-start.2
  96.2 27.1 %collective-permute-start.1 = (bf16[128,2,64]{0,2,1:T(8,128)(2,1)S(1)}, bf16[128,2,64]{0,2,1:T(8,128)(2,1)S(1)}, u32[]{:S(2)}, u32[]{:S(2)}) collective-permute-start(bf16[128,2,64]{0,2,1:T(8,128)(2,1)S(1)} %bitcast.117), channel_id=1, source_target_pairs={{0,4},{4,8},{8,12},{12,16},{16,20},{20,24},{24,28},{28,32},{32,36}... | collective-permute-start | bytes 98312 | tf_op jit(solution)/shard_map/ppermute | solution.py:175
  100.5 5.4 %slice-start = ((s8[7340032]{0:T(1024)(128)(4,1)}), s8[4194304]{0:T(1024)(128)(4,1)S(1)}, s32[]{:S(2)}) async-start(s8[7340032]{0:T(1024)(128)(4,1)} %bitcast.155), calls=%async_computation.2 | async-start | bytes 8388608
  100.6 5.4 %slice-start.1 = ((s8[7340032]{0:T(1024)(128)(4,1)}), s8[3145728]{0:T(1024)(128)(4,1)S(1)}, s32[]{:S(2)}) async-start(s8[7340032]{0:T(1024)(128)(4,1)} %bitcast.155), calls=%async_computation.3 | async-start | bytes 6291456
  100.6 21.5 %collective-permute-start.2 = (bf16[128,2,64]{0,2,1:T(8,128)(2,1)S(1)}, bf16[128,2,64]{0,2,1:T(8,128)(2,1)S(1)}, u32[]{:S(2)}, u32[]{:S(2)}) collective-permute-start(bf16[128,2,64]{0,2,1:T(8,128)(2,1)S(1)} %pad_maximum_fusion.3), channel_id=1, source_target_pairs={{0,4},{4,8},{8,12},{12,16},{16,20},{20,24},{24,28},{28,32},{32,36}... | collective-permute-start | bytes 98312 | tf_op jit(solution)/shard_map/ppermute | solution.py:175
  107.3 4.9 %collective-permute-start = (bf16[30,512]{1,0:T(8,128)(2,1)S(1)}, bf16[30,512]{1,0:T(8,128)(2,1)S(1)}, u32[]{:S(2)}, u32[]{:S(2)}) collective-permute-start(bf16[30,512]{1,0:T(8,128)(2,1)S(1)} %slice.319), channel_id=1, source_target_pairs={{0,4},{4,8},{8,12},{12,16},{16,20},{20,24},{24,28},{28,32},{32,36}... | collective-permute-start | bytes 92168 | tf_op jit(solution)/shard_map/ppermute | solution.py:175
  109.6 1.6 %copy-start.3 = (f32[31,512]{1,0:T(8,128)S(1)}, f32[31,512]{1,0:T(8,128)}, u32[]{:S(2)}) copy-start(f32[31,512]{1,0:T(8,128)} %param.19) | copy-start | bytes 190468
  109.6 2.2 %copy-start.6 = (f32[8]{0:T(128)S(1)}, f32[8]{0:T(128)}, u32[]{:S(2)}) copy-start(f32[8]{0:T(128)} %param.21) | copy-start | bytes 100
  118.1 8.2 %all-to-all-start = ((f32[4,1,1024]{2,1,0:T(1,128)}), f32[4,1,1024]{2,1,0:T(1,128)S(1)}, u32[]{:S(2)}, u32[]{:S(2)}) async-start(f32[4,1,1024]{2,1,0:T(1,128)} %broadcast_in_dim.14), calls=%async_computation | async-start | bytes 32768 | tf_op jit(solution)/shard_map/all_to_all | solution.py:180
  123.2 3.1 %copy-start.5 = (f32[512]{0:T(512)S(1)}, f32[512]{0:T(512)}, u32[]{:S(2)}) copy-start(f32[512]{0:T(512)} %param.20) | copy-start | bytes 6148
  123.3 6.2 %copy-start.4 = (f32[4,2,4,128]{3,2,1,0:T(4,128)}, f32[4,2,4,128]{3,2,1,0:T(4,128)S(1)}, u32[]{:S(2)}) copy-start(f32[4,2,4,128]{3,2,1,0:T(4,128)S(1)} %add_log_fusion) | copy-start | bytes 49156
  126.3 3.2 %copy-start.1 = (bf16[8,8,2,16,1024]{4,3,2,1,0:T(8,128)(2,1)S(1)}, bf16[8,8,2,16,1024]{4,3,2,1,0:T(8,128)(2,1)}, u32[]{:S(2)}) copy-start(bf16[8,8,2,16,1024]{4,3,2,1,0:T(8,128)(2,1)} %get-tuple-element.5) | copy-start | bytes 12582916

commit v2 on v0

v2 whole, which is shorter than its diff:
```python
import jax
import jax.numpy as jnp
from jax import lax
from jax.experimental import pallas as pl
from jax.experimental.pallas import tpu as pltpu
from jax.sharding import PartitionSpec as P

CONV_CH = 2048
HEADS = 32
KV_HEADS = 8
HEAD_DIM = 64
WINDOW = 128
NORM_EPS = 1e-06
CHANNEL_EPS = 1e-05
ROPE_BASE = 10000.0
MESH = pl.DeviceIdType.MESH
F32 = jnp.float32
BF16 = jnp.bfloat16

SIDE = 8
TP = 4
ROWS = 512
WIDTH = 2048
GROUPS = ((0, 1792), (1792, 2816))
ORDER = (0, 1, -1, 2, -2, 3, -3, 4)
NT = (((1,), (1,)), ((), ()))


def kernel(
    tokens_ref,
    gain_ref,
    wcv_ref,
    wcg_ref,
    wq_ref,
    wk_ref,
    wv_ref,
    taps_ref,
    lng_ref,
    sinks_ref,
    oc_ref,
    oa_ref,
    cos_ref,
    sin_ref,
    mixed_ref,
    logs_ref,
    full,
    piece,
    tok,
    normed,
    raw,
    ext,
    conv,
    sums,
    q_buf,
    kz,
    vz,
    act,
    halo_send,
    halo_recv,
    glu_send,
    glu_recv,
    stat_send,
    stat_recv,
    part,
    relay_in,
    relay_out,
    from_low,
    from_high,
    tok_sem,
    drecv,
    dsend,
    rrecv,
    rsend,
    precv,
    psend,
    hsend,
    hrecv,
    ssend,
    srecv,
    xsend,
    xrecv,
):
    me = lax.axis_index("sp")
    x = lax.axis_index("tp")
    core = lax.rem(me, 2)
    y = lax.rem(me // 2, SIDE)
    z = me // (2 * SIDE)

    def device(zz, yy, cc):
        return {"sp": (zz * SIDE + yy) * 2 + cc}

    def wrap(v):
        return lax.rem(v + 2 * SIDE, SIDE)

    def at(a, b, c):
        return wrap(z + (1 - c) * a + c * b), wrap(y + (1 - c) * b + c * a)

    def peer(a, b):
        return device(*at(a, b, core), core)

    def across(d):
        return {"tp": lax.rem(x + d + TP, TP)}

    partner = device(z, y, 1 - core)
    count = 2 * SIDE * SIDE
    after = {"sp": lax.rem(me + 1, count)}
    before = {"sp": lax.rem(me + count - 1, count)}
    started = []

    def remote(src, dst, send, recv, to):
        return pltpu.make_async_remote_copy(
            src_ref=src,
            dst_ref=dst,
            send_sem=send,
            recv_sem=recv,
            device_id=to,
            device_id_type=MESH,
        )

    def go(src, dst, send, recv, to):
        copy = remote(src, dst, send, recv, to)
        copy.start()
        started.append(copy)

    tok_copy = pltpu.make_async_copy(tokens_ref, tok, tok_sem)
    tok_copy.start()
    piece[:, 0:512] = wcv_ref[...]
    piece[:, 512:1024] = wcg_ref[...]
    piece[:, 1024:1536] = wq_ref[...]
    piece[:, 1536:1664] = wk_ref[...]
    piece[:, 1664:1792] = wv_ref[...]
    piece[:, 1792:2304] = oc_ref[...]
    piece[:, 2304:2816] = oa_ref[...]
    full[pl.ds(pl.multiple_of(me * 16, 16), 16), :] = piece[...]

    greeted = [peer(a, 0) for a in ORDER[1:]] + [peer(0, 1), peer(0, -1), partner]
    greeted += [after, before] + [across(d) for d in (1, 2, 3)]
    barrier = pltpu.get_barrier_semaphore()
    for one in greeted:
        pl.semaphore_signal(barrier, inc=1, device_id=one, device_id_type=MESH)
    pl.semaphore_wait(barrier, len(greeted))

    def slot(g, a, b, c=None, half=None):
        c = core if c is None else c
        zz, yy = at(-a, -b, c)
        low, high = GROUPS[g]
        width = high - low
        if half is not None:
            width = width // 2
            low = low + half * width
        row = pl.multiple_of(((zz * SIDE + yy) * 2 + c) * 16, 16)
        return full.at[pl.ds(row, 16), pl.ds(low, width)]

    def own(g):
        low, high = GROUPS[g]
        return piece.at[:, pl.ds(low, high - low)]

    def direct(g):
        for i, a in enumerate(ORDER):
            if a:
                go(own(g), slot(g, 0, 0), dsend.at[g, i], drecv.at[g, i], peer(a, 0))

    def arrived(ref, sem):
        remote(ref, ref, hsend.at[0], sem, partner).wait_recv()

    def to_partner(g, i, a, b):
        ref = slot(g, a, b)
        go(own(g) if a == b == 0 else ref, ref, psend.at[g, i, b + 3], precv.at[g, i, b + 3], partner)

    def batch(g, s):
        for i, a in enumerate(ORDER):
            if s == 0:
                ref = slot(g, a, 0)
                if a:
                    arrived(ref, drecv.at[g, i])
                src = ref if a else own(g)
                go(src, ref, rsend.at[g, i, 3], rrecv.at[g, i, 4], peer(0, 1))
                go(src, ref, rsend.at[g, i, 4], rrecv.at[g, i, 2], peer(0, -1))
                to_partner(g, i, a, 0)
            elif s < 4:
                for sign in (1, -1):
                    ref = slot(g, a, sign * s)
                    arrived(ref, rrecv.at[g, i, 3 + sign * s])
                    if s < 3:
                        b = sign * (s + 1)
                        lane = 4 + s if sign > 0 else 3 - s
                        go(ref, ref, rsend.at[g, i, lane], rrecv.at[g, i, 3 + b], peer(0, sign))
                    else:
                        h = 0 if sign > 0 else 1
                        ref = slot(g, a, sign * s, half=h)
                        lane = 7 if sign > 0 else 0
                        go(ref, ref, rsend.at[g, i, lane], rrecv.at[g, i, 7 + h], peer(0, sign))
                    to_partner(g, i, a, sign * s)
            else:
                for h in range(2):
                    arrived(slot(g, a, 4, half=h), rrecv.at[g, i, 7 + h])
                to_partner(g, i, a, 4)

    def from_partner(g):
        for i, a in enumerate(ORDER):
            for b in ORDER:
                arrived(slot(g, a, b, 1 - core), precv.at[g, i, b + 3])

    def norm_rows(t, carry):
        rows = pl.ds(pl.multiple_of(t * 32, 32), 32)
        v = tok[rows, :].astype(F32)
        scale = lax.rsqrt(jnp.mean(v * v, axis=-1, keepdims=True) + NORM_EPS)
        normed[rows, :] = (v * scale * gain_ref[...].astype(F32)).astype(BF16)
        return carry

    def project(t, carry):
        cols = pl.ds(pl.multiple_of(t * 256, 256), 256)
        raw[:, cols] = jnp.dot(
            normed[...], full[:, cols], preferred_element_type=F32
        ).astype(BF16)
        return carry

    def glu_rows(t, carry):
        rows = pl.ds(pl.multiple_of(t * 64, 64), 64)
        into = pl.ds(pl.multiple_of(32 + t * 64, 32), 64)
        for c in range(4):
            value = raw[rows, c * 128 : (c + 1) * 128].astype(F32)
            gate = raw[rows, 512 + c * 128 : 640 + c * 128].astype(F32)
            glu = value * jax.nn.sigmoid(gate)
            ext[c, into, :] = glu.astype(BF16).astype(F32)
        return carry

    lane = lax.broadcasted_iota(jnp.int32, (64, 128), 1)
    low_part = lax.rem(lane, 64) < 32

    def rotated(v, rows):
        other = jnp.where(low_part, pltpu.roll(v, 96, 1), pltpu.roll(v, 32, 1))
        return v * cos_ref[rows, :] + other * sin_ref[rows, :]

    def spread(buf, v, into, wide):
        first = jnp.where(wide < 64, v, 0.0)
        second = jnp.where(wide < 64, 0.0, v)
        buf[0, into, :] = first.astype(BF16)
        buf[1, into, :] = pltpu.roll(first, 64, 1).astype(BF16)
        buf[2, into, :] = pltpu.roll(second, 64, 1).astype(BF16)
        buf[3, into, :] = second.astype(BF16)

    def key_rows(t, carry):
        rows = pl.ds(pl.multiple_of(t * 64, 64), 64)
        into = pl.ds(pl.multiple_of(128 + t * 64, 64), 64)
        key = rotated(raw[rows, 1536:1664].astype(F32), rows).astype(BF16)
        spread(kz, key.astype(F32), into, lane)
        spread(vz, raw[rows, 1664:1792].astype(F32), into, lane)
        keep = pl.ds(pl.multiple_of(t * 64, 64), 64)
        halo_send[0, keep, :] = key
        return carry

    def query_rows(t, carry):
        rows = pl.ds(pl.multiple_of(t * 64, 64), 64)
        for c in range(4):
            cols = slice(1024 + c * 128, 1152 + c * 128)
            turned = rotated(raw[rows, cols].astype(F32), rows)
            q_buf[rows, c * 128 : (c + 1) * 128] = (turned * HEAD_DIM**-0.5).astype(BF16)
        return carry

    def conv_rows(t, carry):
        rows = pl.ds(pl.multiple_of(t * 64, 64), 64)
        first = jnp.zeros((64, 128), F32)
        second = jnp.zeros((64, 128), F32)
        for c in range(4):
            near = ext[c, pl.ds(pl.multiple_of(t * 64, 64), 96), :]
            total = None
            for shift in range(8):
                acc = None
                span = 72 if shift else 64
                for whole in range(0, 40, 8):
                    tap = whole + shift - 2
                    if 0 <= tap < 31:
                        term = taps_ref[tap : tap + 1, c * 128 : (c + 1) * 128] * near[whole : whole + span]
                        acc = term if acc is None else acc + term
                acc = acc[shift : shift + 64]
                total = acc if total is None else total + acc
            conv[c, rows, :] = total
            first = first + total
            second = second + total * total
        sums[0, rows, :] = first
        sums[1, rows, :] = second
        return carry

    def branch_rows(t, carry):
        rows = pl.ds(pl.multiple_of(t * 64, 64), 64)
        mean = sums[0, rows, :]
        scale = sums[1, rows, :]
        for c in range(4):
            cols = slice(c * 128, (c + 1) * 128)
            v = (conv[c, rows, :] - mean) * scale * lng_ref[0:1, cols]
            act[rows, cols] = (v * jax.nn.sigmoid(v)).astype(BF16)
        return carry

    seen = lax.broadcasted_iota(jnp.int32, (128, 256), 1)
    asks = lax.broadcasted_iota(jnp.int32, (128, 256), 0)
    head_lane = lax.broadcasted_iota(jnp.int32, (128, 128), 1)

    def attend(t, carry):
        rows = pl.ds(pl.multiple_of(t * 128, 128), 128)
        window = pl.ds(pl.multiple_of(t * 128, 128), 256)
        least = jnp.where(me * SIDE + t == 0, WINDOW, 0)
        allowed = (seen > asks) & (seen <= asks + WINDOW) & (seen >= least)
        logs = jnp.zeros((128, 128), F32)
        for pair in range(4):
            q = q_buf[rows, pair * 128 : (pair + 1) * 128]
            out = None
            for odd in range(2):
                head = 2 * pair + odd
                which = 2 * (pair // 2) + odd
                scores = lax.dot_general(q, kz[which, window, :], NT, preferred_element_type=F32)
                weight = jnp.where(allowed, jnp.exp(scores), 0.0)
                total = jnp.sum(weight, axis=1, keepdims=True)
                total = total + jnp.exp(sinks_ref[0:1, head : head + 1])
                logs = jnp.where(head_lane == head, jnp.log(total), logs)
                weight = (weight * (1.0 / total)).astype(BF16)
                term = jnp.dot(weight, vz[which, window, :], preferred_element_type=F32)
                out = term if out is None else out + term
            act[rows, 512 + pair * 128 : 640 + pair * 128] = out.astype(BF16)
        sums[2, rows, :] = logs
        return carry

    direct(0)
    direct(1)
    tok_copy.wait()
    batch(0, 0)
    lax.fori_loop(0, 6, norm_rows, 0)
    batch(0, 1)
    lax.fori_loop(6, 12, norm_rows, 0)
    batch(0, 2)
    lax.fori_loop(12, 16, norm_rows, 0)
    batch(0, 3)
    batch(1, 0)
    batch(0, 4)
    batch(1, 1)
    from_partner(0)

    lax.fori_loop(0, 4, project, 0)
    batch(1, 2)
    lax.fori_loop(0, 8, glu_rows, 0)
    for c in range(4):
        glu_send[:, c * 128 : (c + 1) * 128] = ext[c, 512:544, :].astype(BF16)
    lax.fori_loop(4, 7, project, 0)
    go(glu_send, glu_recv, hsend.at[0], hrecv.at[0], after)
    batch(1, 3)
    lax.fori_loop(0, 8, key_rows, 0)
    halo_send[1, 384:512, :] = raw[384:512, 1664:1792]
    lax.fori_loop(0, 8, query_rows, 0)
    tail = pl.ds(384, 128)
    go(halo_send.at[0, tail], halo_recv.at[0], hsend.at[1], hrecv.at[1], after)
    go(halo_send.at[1, tail], halo_recv.at[1], hsend.at[2], hrecv.at[2], after)
    batch(1, 4)
    arrived(glu_recv, hrecv.at[0])
    keep = jnp.where(me == 0, 0.0, 1.0).astype(F32)
    for c in range(4):
        ext[c, 0:32, :] = glu_recv[:, c * 128 : (c + 1) * 128].astype(F32) * keep
    lax.fori_loop(0, 8, conv_rows, 0)
    stat_send[...] = jnp.zeros((8, ROWS), F32)
    stat_send[0:1, :] = jnp.sum(sums[0].T, axis=0, keepdims=True)
    stat_send[1:2, :] = jnp.sum(sums[1].T, axis=0, keepdims=True)
    for d in (1, 2, 3):
        go(stat_send, stat_recv.at[d - 1], ssend.at[d - 1], srecv.at[d - 1], across(d))
    arrived(halo_recv.at[0], hrecv.at[1])
    arrived(halo_recv.at[1], hrecv.at[2])
    for t in range(2):
        rows = slice(t * 64, t * 64 + 64)
        spread(kz, halo_recv[0, rows, :].astype(F32), rows, lane)
        spread(vz, halo_recv[1, rows, :].astype(F32), rows, lane)
    lax.fori_loop(0, 4, attend, 0)
    logs_ref[...] = sums[2].T[0:8, :]
    for d in range(3):
        arrived(stat_recv.at[d], srecv.at[d])
    stats = stat_send[0:2, :] + stat_recv[0, 0:2, :] + stat_recv[1, 0:2, :] + stat_recv[2, 0:2, :]
    stats = stats / CONV_CH
    mean = stats[0:1, :]
    scale = lax.rsqrt(stats[1:2, :] - mean * mean + CHANNEL_EPS)
    sums[0] = jnp.broadcast_to(mean, (128, ROWS)).T
    sums[1] = jnp.broadcast_to(scale, (128, ROWS)).T
    lax.fori_loop(0, 8, branch_rows, 0)
    from_partner(1)

    def rows_of(d):
        return pl.ds(pl.multiple_of(lax.rem(x + d + TP, TP) * 128, 128), 128)

    def out_part(n):
        def one(t, carry):
            cols = pl.ds(pl.multiple_of(t * 256, 256), 256)
            wrows = pl.ds(pl.multiple_of(n * 512 + t * 256, 256), 256)
            part[n, :, cols] = lax.dot_general(
                act[...], full[wrows, 1792:2816], NT, preferred_element_type=F32
            ).astype(BF16)
            return carry

        lax.fori_loop(0, 2, one, 0)

    inbox = {1: from_low, -1: from_high}
    for n in (0, 2, 1, 3):
        out_part(n)
        far = 1 if n < 2 else -1
        go(part.at[n, rows_of(2)], relay_in.at[n], xsend.at[0, n], xrecv.at[0, n], across(far))
        go(part.at[n, rows_of(-far)], inbox[-far].at[n], xsend.at[1, n], xrecv.at[1, n], across(-far))
    for n in (0, 2, 1, 3):
        far = 1 if n < 2 else -1
        arrived(relay_in.at[n], xrecv.at[0, n])
        relay_out[n] = (
            part[n, rows_of(far), :].astype(F32) + relay_in[n].astype(F32)
        ).astype(BF16)
        go(relay_out.at[n], inbox[far].at[n], xsend.at[2, n], xrecv.at[2, n], across(far))
    for n in (0, 2, 1, 3):
        arrived(from_low.at[n], xrecv.at[2 if n < 2 else 1, n])
        arrived(from_high.at[n], xrecv.at[1 if n < 2 else 2, n])
        mixed_ref[:, n * 512 : (n + 1) * 512] = (
            part[n, rows_of(0), :].astype(F32)
            + from_low[n].astype(F32)
            + from_high[n].astype(F32)
        ).astype(BF16)
    for copy in started:
        copy.wait_send()


def shards(
    tokens,
    norm_gain,
    w_conv_value,
    w_conv_gate,
    w_query,
    w_key,
    w_value,
    conv_taps,
    ln_gain,
    sinks,
    out_conv,
    out_attn,
):
    half_dim = HEAD_DIM // 2
    position = lax.axis_index("sp") * ROWS + lax.broadcasted_iota(jnp.int32, (ROWS, 128), 0)
    which = lax.broadcasted_iota(jnp.int32, (ROWS, 128), 1)
    inverse = ROPE_BASE ** (-(which % half_dim).astype(F32) / half_dim)
    angles = position.astype(F32) * inverse
    cosine = jnp.cos(angles)
    sine = jnp.where(which % HEAD_DIM < half_dim, -1.0, 1.0) * jnp.sin(angles)
    dma = pltpu.SemaphoreType.DMA
    vmem = pl.BlockSpec(memory_space=pltpu.VMEM)
    V = pltpu.VMEM
    return pl.pallas_call(
        kernel,
        out_shape=(
            jax.ShapeDtypeStruct((128, WIDTH), BF16),
            jax.ShapeDtypeStruct((8, ROWS), F32),
        ),
        in_specs=[pl.BlockSpec(memory_space=pl.ANY)] + [vmem] * 13,
        out_specs=(vmem, vmem),
        scratch_shapes=[
            V((WIDTH, 2816), BF16),
            V((16, 2816), BF16),
            V((ROWS, WIDTH), BF16),
            V((ROWS, WIDTH), BF16),
            V((ROWS, 1792), BF16),
            V((4, 544, 128), F32),
            V((4, ROWS, 128), F32),
            V((3, ROWS, 128), F32),
            V((ROWS, 512), BF16),
            V((4, 640, 128), BF16),
            V((4, 640, 128), BF16),
            V((ROWS, 1024), BF16),
            V((2, ROWS, 128), BF16),
            V((2, 128, 128), BF16),
            V((32, 512), BF16),
            V((32, 512), BF16),
            V((8, ROWS), F32),
            V((3, 8, ROWS), F32),
            V((4, ROWS, 512), BF16),
            V((4, 128, 512), BF16),
            V((4, 128, 512), BF16),
            V((4, 128, 512), BF16),
            V((4, 128, 512), BF16),
            dma,
            dma((2, 8)),
            dma((2, 8)),
            dma((2, 8, 9)),
            dma((2, 8, 8)),
            dma((2, 8, 8)),
            dma((2, 8, 8)),
            dma((3,)),
            dma((3,)),
            dma((3,)),
            dma((3,)),
            dma((3, 4)),
            dma((3, 4)),
        ],
        compiler_params=pltpu.CompilerParams(collective_id=0, has_side_effects=True),
        name="layer",
    )(
        tokens,
        norm_gain.reshape(1, WIDTH),
        w_conv_value,
        w_conv_gate,
        w_query,
        w_key,
        w_value,
        conv_taps,
        ln_gain.reshape(1, 512),
        sinks.reshape(1, 8),
        out_conv.T,
        out_attn.T,
        cosine,
        sine,
    )


def solution(mesh):
    in_specs = (
        P("sp", None),
        P(),
        P("sp", "tp"),
        P("sp", "tp"),
        P("sp", "tp"),
        P("sp", "tp"),
        P("sp", "tp"),
        P(None, "tp"),
        P("tp"),
        P("tp"),
        P("tp", "sp"),
        P("tp", "sp"),
    )
    out_specs = (P(("sp", "tp"), None), P("tp", "sp"))
    return jax.shard_map(shards, mesh=mesh, in_specs=in_specs, out_specs=out_specs, check_vma=False)
```

time: 232 us -> 101 us (0.44)
  waiting for transfers between devices: 136 us -> 0 us
  Pallas kernels: 0 us -> 93.5 us
  blocking collectives: 29.6 us -> 0 us
  matrix products: 16.9 us -> 0 us
  between operations: 14.5 us -> 0.67 us
  starting transfers between devices: 12.9 us -> 0 us
  other arithmetic: 11.8 us -> 1.82 us
  local copies, waits for them, and re-layouts: 9.71 us -> 4.5 us
    all_gather x2 -> x0, waiting for transfers between devices: 134 us -> none  [the longest x1 84.2 us: sent_together(): whole = lax.all_gather(both, axis, axis=dim, tiled=True)]
    pallas_call x0 -> x1, Pallas kernels: none -> 93.5 us  [shards(): pl.pallas_call(kernel, out_shape=(jax.ShapeDtypeStruct((128, WIDTH), BF16...]
    all_to_all x1 -> x0, blocking collectives: 29.6 us -> none  [summed_on_arrival(): lax.all_to_all(pieces, axis, split_axis=0, concat_axis=0, tiled=True)]
    dot_general x9 -> x0, matrix products: 16.9 us -> none  [the longest x5 10.4 us: shards(): jnp.dot(normed, piece, preferred_element_type=jnp.float32)]
    ppermute x3 -> x0, starting transfers between devices: 8.87 us -> none  [shifted(): lax.ppermute(value, axis, [(source, source + steps) for source in range(i...]
    reduce_sum x4 -> x0, other arithmetic: 8.46 us -> none  [the longest x1 5.05 us: shards(): sum_first = jnp.sum(conv_out, axis=-1)]
    all_to_all x1 -> x0, starting transfers between devices: 3.97 us -> none  [from_everyone(): lax.all_to_all(jnp.broadcast_to(shard[None], (peers, *shard.shape)), axis...]
    slice x6 -> x0, local copies, waits for them, and re-layouts: 2.83 us -> none  [the longest x2 2.76 us: shards(): conv_taps[tap][None, :] * extended[tap:tap + row_count]]
  transfers between devices with their start and end apart: 6 -> 0, of which waited for: 3 -> 0; matrix products, arithmetic and copies ran while one was open for 12% -> 0% of each run, Pallas kernels for 0% -> 0%
where the time goes in v2:
time: 101 us
  Pallas kernels  93.5 us (93%)
  local copies, waits for them, and re-layouts  4.5 us (4%)
  other arithmetic  1.82 us (2%)
    pallas_call x1, Pallas kernels, shards(): pl.pallas_call(kernel, out_shape=(jax.ShapeDtypeStruct((128, WIDTH), BF16...  93.5 us
    unnamed x2, local copies, waits for them, and re-layouts  3.2 us

profile of v2, /device:TPU:1, one launch (start us, length us, event | category | flops | bytes accessed | tf_op | source)
XLA Modules:
  0.0 100.5 jit_solution(14144549560709883294)
XLA Ops:
  0.7 1.3 %reshape.13.gain_ref = bf16[1,2048]{1,0:T(2,128)(2,1)} reshape(bf16[2048]{0:T(1024)(128)(2,1)} %param.13) | data formatting | bytes 8192 | tf_op jit(solution)/shard_map/reshape | solution.py:495
  2.0 1.8 %sine_multiply_fusion = (f32[512,128]{1,0:T(8,128)}, f32[512,128]{1,0:T(8,128)}) fusion(s32[128]{0:T(128)S(1)} %get-tuple-element.6, s32[128]{0:T(128)S(1)} %get-tuple-element.8, s32[128]{0:T(128)S(1)} %get-tuple-element.7, s32[128]{0:T(128)S(1)} %get-tuple-element.9, f32[512]{0:T(512)S(1)} %add_convert_fusion, pred[128]{0:T(512)(128)(4,1)S(1)} %get-tuple-element.4, ...), kind=kLoop, calls=%fused_computation | loop fusion | flops 589824 | bytes 528640 | tf_op jit(solution)/shard_map/mul | solution.py:441
  3.8 93.5 %layer.1 = (bf16[128,2048]{1,0:T(8,128)(2,1)}, f32[8,512]{1,0:T(8,128)}) custom-call(bf16[512,2048]{1,0:T(8,128)(2,1)} %tokens_ref.1, bf16[1,2048]{1,0:T(2,128)(2,1)} %reshape.13.gain_ref, bf16[16,512]{1,0:T(8,128)(2,1)} %wcv_ref.1, bf16[16,512]{1,0:T(8,128)(2,1)} %wcg_ref.1, bf16[16,512]{1,0:T(8,128)(2,1)} %wq_ref.1, bf16[16,128]{1,0:T(8,128)(2,1)} %wk_ref.1, ...), custom_call_target="tpu_custom_call" | custom-call | tf_op jit(solution)/shard_map/layer/pallas_call | solution.py:445
  97.3 1.9 %copy.16 = bf16[128,2048]{1,0:T(8,128)(2,1)} copy(bf16[128,2048]{1,0:T(8,128)(2,1)} %get-tuple-element.12) | data formatting | bytes 1048576
  99.2 1.3 %copy.17 = f32[8,512]{1,0:T(8,128)} copy(f32[8,512]{1,0:T(8,128)} %get-tuple-element.13) | data formatting | bytes 32768
  (4 shorter events, 0.0 us)

commit v3 on v2

--- a/solution.py
+++ b/solution.py
@@ -1,5 +1,6 @@
 import jax
 import jax.numpy as jnp
+import numpy as np
 from jax import lax
 from jax.experimental import pallas as pl
 from jax.experimental.pallas import tpu as pltpu
@@ -21,7 +22,7 @@
 TP = 4
 ROWS = 512
 WIDTH = 2048
-GROUPS = ((0, 1792), (1792, 2816))
+GROUPS = ((0, 1024), (1024, 1792), (1792, 2816))
 ORDER = (0, 1, -1, 2, -2, 3, -3, 4)
 NT = (((1,), (1,)), ((), ()))
 
@@ -39,8 +40,7 @@
     sinks_ref,
     oc_ref,
     oa_ref,
-    cos_ref,
-    sin_ref,
+    inv_ref,
     mixed_ref,
     logs_ref,
     full,
@@ -68,17 +68,17 @@
     from_high,
     tok_sem,
     drecv,
-    dsend,
     rrecv,
-    rsend,
     precv,
-    psend,
+    gsend,
     hsend,
     hrecv,
     ssend,
     srecv,
     xsend,
     xrecv,
+    cos_ref,
+    sin_ref,
 ):
     me = lax.axis_index("sp")
     x = lax.axis_index("tp")
@@ -158,54 +158,70 @@
     def direct(g):
         for i, a in enumerate(ORDER):
             if a:
-                go(own(g), slot(g, 0, 0), dsend.at[g, i], drecv.at[g, i], peer(a, 0))
+                remote(own(g), slot(g, 0, 0), gsend.at[g], drecv.at[g, i], peer(a, 0)).start()
 
     def arrived(ref, sem):
         remote(ref, ref, hsend.at[0], sem, partner).wait_recv()
 
-    def to_partner(g, i, a, b):
-        ref = slot(g, a, b)
-        go(own(g) if a == b == 0 else ref, ref, psend.at[g, i, b + 3], precv.at[g, i, b + 3], partner)
-
-    def batch(g, s):
-        for i, a in enumerate(ORDER):
-            if s == 0:
-                ref = slot(g, a, 0)
-                if a:
-                    arrived(ref, drecv.at[g, i])
-                src = ref if a else own(g)
-                go(src, ref, rsend.at[g, i, 3], rrecv.at[g, i, 4], peer(0, 1))
-                go(src, ref, rsend.at[g, i, 4], rrecv.at[g, i, 2], peer(0, -1))
-                to_partner(g, i, a, 0)
-            elif s < 4:
-                for sign in (1, -1):
-                    ref = slot(g, a, sign * s)
-                    arrived(ref, rrecv.at[g, i, 3 + sign * s])
-                    if s < 3:
-                        b = sign * (s + 1)
-                        lane = 4 + s if sign > 0 else 3 - s
-                        go(ref, ref, rsend.at[g, i, lane], rrecv.at[g, i, 3 + b], peer(0, sign))
-                    else:
-                        h = 0 if sign > 0 else 1
-                        ref = slot(g, a, sign * s, half=h)
-                        lane = 7 if sign > 0 else 0
-                        go(ref, ref, rsend.at[g, i, lane], rrecv.at[g, i, 7 + h], peer(0, sign))
-                    to_partner(g, i, a, sign * s)
-            else:
-                for h in range(2):
-                    arrived(slot(g, a, 4, half=h), rrecv.at[g, i, 7 + h])
-                to_partner(g, i, a, 4)
+    def place(i):
+        if isinstance(i, int):
+            return ORDER[i]
+        return (i + 1) // 2 * (2 * lax.rem(i, 2) - 1)
+
+    def serve(g, s, i):
+        a = place(i)
+
+        def ring(src, ref, b, recv):
+            remote(src, ref, gsend.at[g], recv, peer(0, 1 if b > 0 else -1)).start()
+
+        def share(src, ref):
+            remote(src, ref, gsend.at[g], precv.at[g], partner).start()
+
+        if s == 0:
+            ref = slot(g, a, 0)
+            if a:
+                arrived(ref, drecv.at[g, i])
+            src = ref if a else own(g)
+            for b in (1, -1):
+                ring(src, ref, b, rrecv.at[g, i, 3 + b])
+            share(src, ref)
+        elif s < 4:
+            for sign in (1, -1):
+                ref = slot(g, a, sign * s)
+                arrived(ref, rrecv.at[g, i, 3 + sign * s])
+                if s < 3:
+                    b = sign * (s + 1)
+                    ring(ref, ref, b, rrecv.at[g, i, 3 + b])
+                else:
+                    h = 0 if sign > 0 else 1
+                    out = slot(g, a, sign * s, half=h)
+                    ring(out, out, sign, rrecv.at[g, i, 7 + h])
+                share(ref, ref)
+        else:
+            for h in range(2):
+                arrived(slot(g, a, 4, half=h), rrecv.at[g, i, 7 + h])
+            share(slot(g, a, 4), slot(g, a, 4))
+
+    def batch(g, s, items=range(8)):
+        for i in items:
+            serve(g, s, i)
+
+    def rows_in(g, count):
+        low, high = GROUPS[g]
+        return full.at[pl.ds(0, count), pl.ds(low, high - low)]
 
     def from_partner(g):
-        for i, a in enumerate(ORDER):
-            for b in ORDER:
-                arrived(slot(g, a, b, 1 - core), precv.at[g, i, b + 3])
+        arrived(rows_in(g, 1024), precv.at[g])
+
+    def sent(g):
+        ref = rows_in(g, 127 * 16)
+        remote(ref, ref, gsend.at[g], tok_sem, partner).wait_send()
 
     def norm_rows(t, carry):
         rows = pl.ds(pl.multiple_of(t * 32, 32), 32)
         v = tok[rows, :].astype(F32)
         scale = lax.rsqrt(jnp.mean(v * v, axis=-1, keepdims=True) + NORM_EPS)
-        normed[rows, :] = (v * scale * gain_ref[...].astype(F32)).astype(BF16)
+        normed[rows, :] = (v * scale * gain_ref[...].astype(F32).reshape(1, WIDTH)).astype(BF16)
         return carry
 
     def project(t, carry):
@@ -227,6 +243,15 @@
 
     lane = lax.broadcasted_iota(jnp.int32, (64, 128), 1)
     low_part = lax.rem(lane, 64) < 32
+
+    def table_rows(t, carry):
+        rows = pl.ds(pl.multiple_of(t * 64, 64), 64)
+        position = me * ROWS + t * 64 + lax.broadcasted_iota(jnp.int32, (64, 128), 0)
+        angle = position.astype(F32) * inv_ref[...]
+        sine = jnp.sin(angle)
+        cos_ref[rows, :] = jnp.cos(angle)
+        sin_ref[rows, :] = jnp.where(low_part, -sine, sine)
+        return carry
 
     def rotated(v, rows):
         other = jnp.where(low_part, pltpu.roll(v, 96, 1), pltpu.roll(v, 32, 1))
@@ -320,54 +345,109 @@
         sums[2, rows, :] = logs
         return carry
 
+    def each(body, g, s, per, start=0):
+        def both(t, carry):
+            carry = body(t, carry)
+            for k in range(per):
+                serve(g, s, (t - start) * per + k)
+            return carry
+
+        return both
+
+    batch(0, 0, (0,))
     direct(0)
+    batch(1, 0, (0,))
     direct(1)
+    lax.fori_loop(0, 8, table_rows, 0)
     tok_copy.wait()
-    batch(0, 0)
-    lax.fori_loop(0, 6, norm_rows, 0)
+    batch(0, 0, range(1, 8))
+    lax.fori_loop(0, 5, norm_rows, 0)
     batch(0, 1)
-    lax.fori_loop(6, 12, norm_rows, 0)
+    batch(1, 0, range(1, 8))
+    lax.fori_loop(5, 10, norm_rows, 0)
     batch(0, 2)
-    lax.fori_loop(12, 16, norm_rows, 0)
+    batch(1, 1)
+    batch(2, 0, (0,))
+    direct(2)
+    lax.fori_loop(10, 16, norm_rows, 0)
     batch(0, 3)
-    batch(1, 0)
+    batch(1, 2)
+    batch(2, 0, range(1, 8))
     batch(0, 4)
-    batch(1, 1)
+    batch(1, 3)
+    batch(2, 1)
     from_partner(0)
 
-    lax.fori_loop(0, 4, project, 0)
-    batch(1, 2)
-    lax.fori_loop(0, 8, glu_rows, 0)
+    lax.fori_loop(0, 2, project, 0)
+    lax.fori_loop(2, 4, each(project, 1, 4, 4, 2), 0)
+    lax.fori_loop(0, 8, each(glu_rows, 2, 2, 1), 0)
     for c in range(4):
         glu_send[:, c * 128 : (c + 1) * 128] = ext[c, 512:544, :].astype(BF16)
+    lax.fori_loop(1, 4, conv_rows, 0)
+    go(glu_send, glu_recv, hsend.at[0], hrecv.at[0], after)
+    lax.fori_loop(4, 8, conv_rows, 0)
+    from_partner(1)
     lax.fori_loop(4, 7, project, 0)
-    go(glu_send, glu_recv, hsend.at[0], hrecv.at[0], after)
-    batch(1, 3)
-    lax.fori_loop(0, 8, key_rows, 0)
+    lax.fori_loop(0, 8, each(key_rows, 2, 3, 1), 0)
     halo_send[1, 384:512, :] = raw[384:512, 1664:1792]
-    lax.fori_loop(0, 8, query_rows, 0)
-    tail = pl.ds(384, 128)
-    go(halo_send.at[0, tail], halo_recv.at[0], hsend.at[1], hrecv.at[1], after)
-    go(halo_send.at[1, tail], halo_recv.at[1], hsend.at[2], hrecv.at[2], after)
-    batch(1, 4)
     arrived(glu_recv, hrecv.at[0])
     keep = jnp.where(me == 0, 0.0, 1.0).astype(F32)
     for c in range(4):
         ext[c, 0:32, :] = glu_recv[:, c * 128 : (c + 1) * 128].astype(F32) * keep
-    lax.fori_loop(0, 8, conv_rows, 0)
+    tail = pl.ds(384, 128)
+    go(halo_send.at[0, tail], halo_recv.at[0], hsend.at[1], hrecv.at[1], after)
+    go(halo_send.at[1, tail], halo_recv.at[1], hsend.at[2], hrecv.at[2], after)
+    lax.fori_loop(0, 1, conv_rows, 0)
     stat_send[...] = jnp.zeros((8, ROWS), F32)
     stat_send[0:1, :] = jnp.sum(sums[0].T, axis=0, keepdims=True)
     stat_send[1:2, :] = jnp.sum(sums[1].T, axis=0, keepdims=True)
     for d in (1, 2, 3):
         go(stat_send, stat_recv.at[d - 1], ssend.at[d - 1], srecv.at[d - 1], across(d))
+    lax.fori_loop(0, 8, each(query_rows, 2, 4, 1), 0)
     arrived(halo_recv.at[0], hrecv.at[1])
     arrived(halo_recv.at[1], hrecv.at[2])
     for t in range(2):
         rows = slice(t * 64, t * 64 + 64)
         spread(kz, halo_recv[0, rows, :].astype(F32), rows, lane)
         spread(vz, halo_recv[1, rows, :].astype(F32), rows, lane)
-    lax.fori_loop(0, 4, attend, 0)
-    logs_ref[...] = sums[2].T[0:8, :]
+
+    def block(d):
+        return lax.rem(x + d + TP, TP)
+
+    def rows_of(d):
+        return pl.ds(pl.multiple_of(block(d) * 128, 128), 128)
+
+    def out_part(d, chunks):
+        for n in chunks:
+            part[n, rows_of(d), :] = lax.dot_general(
+                act[rows_of(d), :],
+                full[n * 512 : (n + 1) * 512, 1792:2816],
+                NT,
+                preferred_element_type=F32,
+            ).astype(BF16)
+
+    def branch(d):
+        lax.fori_loop(2 * block(d), 2 * block(d) + 2, branch_rows, 0)
+
+    inbox = {1: from_low, -1: from_high}
+
+    def send_far(n):
+        far = 1 if n < 2 else -1
+        go(part.at[n, rows_of(2)], relay_in.at[n], xsend.at[0, n], xrecv.at[0, n], across(far))
+
+    def send_near(n):
+        to = -1 if n < 2 else 1
+        go(part.at[n, rows_of(to)], inbox[to].at[n], xsend.at[1, n], xrecv.at[1, n], across(to))
+
+    def send_relay(n):
+        far = 1 if n < 2 else -1
+        arrived(relay_in.at[n], xrecv.at[0, n])
+        relay_out[n] = (
+            part[n, rows_of(far), :].astype(F32) + relay_in[n].astype(F32)
+        ).astype(BF16)
+        go(relay_out.at[n], inbox[far].at[n], xsend.at[2, n], xrecv.at[2, n], across(far))
+
+    attend(block(2), 0)
     for d in range(3):
         arrived(stat_recv.at[d], srecv.at[d])
     stats = stat_send[0:2, :] + stat_recv[0, 0:2, :] + stat_recv[1, 0:2, :] + stat_recv[2, 0:2, :]
@@ -376,36 +456,31 @@
     scale = lax.rsqrt(stats[1:2, :] - mean * mean + CHANNEL_EPS)
     sums[0] = jnp.broadcast_to(mean, (128, ROWS)).T
     sums[1] = jnp.broadcast_to(scale, (128, ROWS)).T
-    lax.fori_loop(0, 8, branch_rows, 0)
-    from_partner(1)
-
-    def rows_of(d):
-        return pl.ds(pl.multiple_of(lax.rem(x + d + TP, TP) * 128, 128), 128)
-
-    def out_part(n):
-        def one(t, carry):
-            cols = pl.ds(pl.multiple_of(t * 256, 256), 256)
-            wrows = pl.ds(pl.multiple_of(n * 512 + t * 256, 256), 256)
-            part[n, :, cols] = lax.dot_general(
-                act[...], full[wrows, 1792:2816], NT, preferred_element_type=F32
-            ).astype(BF16)
-            return carry
-
-        lax.fori_loop(0, 2, one, 0)
-
-    inbox = {1: from_low, -1: from_high}
+    branch(2)
+    from_partner(2)
     for n in (0, 2, 1, 3):
-        out_part(n)
-        far = 1 if n < 2 else -1
-        go(part.at[n, rows_of(2)], relay_in.at[n], xsend.at[0, n], xrecv.at[0, n], across(far))
-        go(part.at[n, rows_of(-far)], inbox[-far].at[n], xsend.at[1, n], xrecv.at[1, n], across(-far))
-    for n in (0, 2, 1, 3):
-        far = 1 if n < 2 else -1
-        arrived(relay_in.at[n], xrecv.at[0, n])
-        relay_out[n] = (
-            part[n, rows_of(far), :].astype(F32) + relay_in[n].astype(F32)
-        ).astype(BF16)
-        go(relay_out.at[n], inbox[far].at[n], xsend.at[2, n], xrecv.at[2, n], across(far))
+        out_part(2, (n,))
+        send_far(n)
+    attend(block(1), 0)
+    branch(1)
+    for n in (2, 3):
+        out_part(1, (n,))
+        send_near(n)
+    attend(block(-1), 0)
+    branch(-1)
+    for n in (0, 1):
+        out_part(-1, (n,))
+        send_near(n)
+    for n in (0, 1):
+        out_part(1, (n,))
+        send_relay(n)
+    for n in (2, 3):
+        out_part(-1, (n,))
+        send_relay(n)
+    attend(block(0), 0)
+    branch(0)
+    out_part(0, range(4))
+    logs_ref[...] = sums[2].T[0:8, :]
     for n in (0, 2, 1, 3):
         arrived(from_low.at[n], xrecv.at[2 if n < 2 else 1, n])
         arrived(from_high.at[n], xrecv.at[1 if n < 2 else 2, n])
@@ -416,6 +491,13 @@
         ).astype(BF16)
     for copy in started:
         copy.wait_send()
+    for g in range(3):
+        sent(g)
+
+
+def hand_on(mixed_in, logs_in, mixed_out, logs_out):
+    mixed_out[...] = mixed_in[...]
+    logs_out[...] = logs_in[...]
 
 
 def shards(
@@ -433,22 +515,18 @@
     out_attn,
 ):
     half_dim = HEAD_DIM // 2
-    position = lax.axis_index("sp") * ROWS + lax.broadcasted_iota(jnp.int32, (ROWS, 128), 0)
-    which = lax.broadcasted_iota(jnp.int32, (ROWS, 128), 1)
-    inverse = ROPE_BASE ** (-(which % half_dim).astype(F32) / half_dim)
-    angles = position.astype(F32) * inverse
-    cosine = jnp.cos(angles)
-    sine = jnp.where(which % HEAD_DIM < half_dim, -1.0, 1.0) * jnp.sin(angles)
+    inverse = ROPE_BASE ** (-np.arange(half_dim, dtype=np.float32) / half_dim)
+    inverse = jnp.asarray(np.tile(inverse.astype(np.float32), 4)[None, :])
     dma = pltpu.SemaphoreType.DMA
     vmem = pl.BlockSpec(memory_space=pltpu.VMEM)
     V = pltpu.VMEM
-    return pl.pallas_call(
+    mixed, logs = pl.pallas_call(
         kernel,
         out_shape=(
             jax.ShapeDtypeStruct((128, WIDTH), BF16),
             jax.ShapeDtypeStruct((8, ROWS), F32),
         ),
-        in_specs=[pl.BlockSpec(memory_space=pl.ANY)] + [vmem] * 13,
+        in_specs=[pl.BlockSpec(memory_space=pl.ANY)] + [vmem] * 12,
         out_specs=(vmem, vmem),
         scratch_shapes=[
             V((WIDTH, 2816), BF16),
@@ -475,24 +553,24 @@
             V((4, 128, 512), BF16),
             V((4, 128, 512), BF16),
             dma,
-            dma((2, 8)),
-            dma((2, 8)),
-            dma((2, 8, 9)),
-            dma((2, 8, 8)),
-            dma((2, 8, 8)),
-            dma((2, 8, 8)),
+            dma((3, 8)),
+            dma((3, 8, 9)),
+            dma((3,)),
+            dma((3,)),
             dma((3,)),
             dma((3,)),
             dma((3,)),
             dma((3,)),
             dma((3, 4)),
             dma((3, 4)),
+            V((ROWS, 128), F32),
+            V((ROWS, 128), F32),
         ],
         compiler_params=pltpu.CompilerParams(collective_id=0, has_side_effects=True),
         name="layer",
     )(
         tokens,
-        norm_gain.reshape(1, WIDTH),
+        norm_gain,
         w_conv_value,
         w_conv_gate,
         w_query,
@@ -503,9 +581,18 @@
         sinks.reshape(1, 8),
         out_conv.T,
         out_attn.T,
-        cosine,
-        sine,
+        inverse,
     )
+    return pl.pallas_call(
+        hand_on,
+        out_shape=(
+            jax.ShapeDtypeStruct((128, WIDTH), BF16),
+            jax.ShapeDtypeStruct((8, ROWS), F32),
+        ),
+        in_specs=[vmem, vmem],
+        out_specs=(vmem, vmem),
+        name="hand_on",
+    )(mixed, logs)
 
 
 def solution(mesh):

time: 101 us -> 85.9 us (0.85)
  Pallas kernels: 93.5 us -> 85.1 us
  local copies, waits for them, and re-layouts: 4.5 us -> 0 us
  other arithmetic: 1.82 us -> 0 us
    pallas_call x1, Pallas kernels: 93.5 us -> 83.2 us  [shards(): pl.pallas_call(kernel, out_shape=(jax.ShapeDtypeStruct((128, WIDTH), BF16...]
    unnamed x2 -> x0, local copies, waits for them, and re-layouts: 3.2 us -> none
    pallas_call x0 -> x1, Pallas kernels: none -> 1.87 us  [shards(): pl.pallas_call(hand_on, out_shape=(jax.ShapeDtypeStruct((128, WIDTH), BF1...]
    mul x1 -> x0, other arithmetic: 1.8 us -> none  [shards(): sine = jnp.where(which % HEAD_DIM < half_dim, -1.0, 1.0) * jnp.sin(angles)]
    reshape x1 -> x0, local copies, waits for them, and re-layouts: 1.29 us -> none  [shards(): norm_gain.reshape(1, WIDTH)]
where the time goes in v3:
time: 85.9 us; the launch traced here: 85.7 us
  Pallas kernels  85.1 us (99%)
    pallas_call x1, Pallas kernels, shards(): pl.pallas_call(kernel, out_shape=(jax.ShapeDtypeStruct((128, WIDTH), BF16...  83.2 us
    pallas_call x1, Pallas kernels, shards(): pl.pallas_call(hand_on, out_shape=(jax.ShapeDtypeStruct((128, WIDTH), BF1...  1.87 us

profile of v3, /device:TPU:1, one launch (start us, length us, event | category | flops | bytes accessed | tf_op | source)
XLA Modules:
  0.0 85.7 jit_solution(9473417617052095324)
XLA Ops:
  0.6 83.2 %layer.1 = (bf16[128,2048]{1,0:T(8,128)(2,1)}, f32[8,512]{1,0:T(8,128)}) custom-call(bf16[512,2048]{1,0:T(8,128)(2,1)} %tokens_ref.1, bf16[2048]{0:T(1024)(128)(2,1)} %gain_ref.1, bf16[16,512]{1,0:T(8,128)(2,1)} %wcv_ref.1, bf16[16,512]{1,0:T(8,128)(2,1)} %wcg_ref.1, bf16[16,512]{1,0:T(8,128)(2,1)} %wq_ref.1, bf16[16,128]{1,0:T(8,128)(2,1)} %wk_ref.1, ...), custom_call_target="tpu_custom_call" | custom-call | tf_op jit(solution)/shard_map/layer/pallas_call | solution.py:523
  83.8 1.9 %hand_on.1 = (bf16[128,2048]{1,0:T(8,128)(2,1)}, f32[8,512]{1,0:T(8,128)}) custom-call(bf16[128,2048]{1,0:T(8,128)(2,1)} %get-tuple-element.4.mixed_in, f32[8,512]{1,0:T(8,128)} %get-tuple-element.5.logs_in), custom_call_target="tpu_custom_call" | custom-call | tf_op jit(solution)/shard_map/hand_on/pallas_call | solution.py:586

commit v4 on v3

--- a/solution.py
+++ b/solution.py
@@ -374,21 +374,22 @@
     batch(1, 2)
     batch(2, 0, range(1, 8))
     batch(0, 4)
+    from_partner(0)
+
+    lax.fori_loop(0, 2, project, 0)
     batch(1, 3)
     batch(2, 1)
-    from_partner(0)
-
-    lax.fori_loop(0, 2, project, 0)
-    lax.fori_loop(2, 4, each(project, 1, 4, 4, 2), 0)
-    lax.fori_loop(0, 8, each(glu_rows, 2, 2, 1), 0)
+    lax.fori_loop(2, 4, project, 0)
+    lax.fori_loop(0, 8, glu_rows, 0)
     for c in range(4):
         glu_send[:, c * 128 : (c + 1) * 128] = ext[c, 512:544, :].astype(BF16)
     lax.fori_loop(1, 4, conv_rows, 0)
     go(glu_send, glu_recv, hsend.at[0], hrecv.at[0], after)
-    lax.fori_loop(4, 8, conv_rows, 0)
+    lax.fori_loop(4, 8, each(each(conv_rows, 1, 4, 2, 4), 2, 2, 2, 4), 0)
     from_partner(1)
     lax.fori_loop(4, 7, project, 0)
-    lax.fori_loop(0, 8, each(key_rows, 2, 3, 1), 0)
+    batch(2, 3)
+    lax.fori_loop(0, 8, key_rows, 0)
     halo_send[1, 384:512, :] = raw[384:512, 1664:1792]
     arrived(glu_recv, hrecv.at[0])
     keep = jnp.where(me == 0, 0.0, 1.0).astype(F32)

time: 85.9 us -> 85.9 us (level)
  no operation moved by 1% of the time
where the time goes in v4:
time: 85.9 us; the launch traced here: 85.1 us
  Pallas kernels  84.5 us (98%)
    pallas_call x1, Pallas kernels, shards(): pl.pallas_call(kernel, out_shape=(jax.ShapeDtypeStruct((128, WIDTH), BF16...  82.6 us
    pallas_call x1, Pallas kernels, shards(): pl.pallas_call(hand_on, out_shape=(jax.ShapeDtypeStruct((128, WIDTH), BF1...  1.87 us

profile of v4, /device:TPU:1, one launch (start us, length us, event | category | flops | bytes accessed | tf_op | source)
XLA Modules:
  0.0 85.1 jit_solution(16557313142482161721)
XLA Ops:
  0.6 82.6 %layer.1 = (bf16[128,2048]{1,0:T(8,128)(2,1)}, f32[8,512]{1,0:T(8,128)}) custom-call(bf16[512,2048]{1,0:T(8,128)(2,1)} %tokens_ref.1, bf16[2048]{0:T(1024)(128)(2,1)} %gain_ref.1, bf16[16,512]{1,0:T(8,128)(2,1)} %wcv_ref.1, bf16[16,512]{1,0:T(8,128)(2,1)} %wcg_ref.1, bf16[16,512]{1,0:T(8,128)(2,1)} %wq_ref.1, bf16[16,128]{1,0:T(8,128)(2,1)} %wk_ref.1, ...), custom_call_target="tpu_custom_call" | custom-call | tf_op jit(solution)/shard_map/layer/pallas_call | solution.py:524
  83.3 1.9 %hand_on.1 = (bf16[128,2048]{1,0:T(8,128)(2,1)}, f32[8,512]{1,0:T(8,128)}) custom-call(bf16[128,2048]{1,0:T(8,128)(2,1)} %get-tuple-element.4.mixed_in, f32[8,512]{1,0:T(8,128)} %get-tuple-element.5.logs_in), custom_call_target="tpu_custom_call" | custom-call | tf_op jit(solution)/shard_map/hand_on/pallas_call | solution.py:587
